TPU v7x, 512 devices: a 4x2x32 block of a 4x8x32 slice. The times are simulated.
512 devices in a mesh: grp: 2 (over y), fs: 32 (over z), tp: 8 (over x, core).
Axes of the slice: x: 4, y: 2, z: 32, core: 2. Of those that a mesh axis runs over, the one named last changes fastest.
The devices are a block of a 4x8x32 slice.
Arguments:
- tokens: bfloat16 [32768, 2048], P(('grp', 'fs')), parts along dimension 0, may hold values from -6 to 6
- pre_gain: float32 [2048], replicated, may hold values from 0.1 to 1.9
- up_weight: float32 [2048, 8192], P('fs', 'tp'), may hold values from -0.125 to 0.125
- up_scale: float32 [8192], P('tp'), may hold values from 0.3 to 3
- down_weight: float32 [8192, 2048], P('tp', 'fs'), may hold values from -0.0625 to 0.0625
- down_scale: float32 [2048], P('fs'), may hold values from 0.3 to 3
- post_gain: float32 [2048], replicated, may hold values from 0.1 to 1.9
Outputs:
- mixed: bfloat16 [32768, 2048], P(('grp', 'fs')), parts along dimension 0
There are 2 independent parts, one for each index of `grp`. A program takes and returns all parts, laid end to end along the dimension named above; an argument that names none is the same for every part. Nothing has to cross between parts.
All inputs are finite; a program needn't handle non-finite values.
Results may differ from a plain program's by a relative error of at most 0.01.
Values may be sent and summed in bfloat16 or wider, within the bound.
A program may use at most 64 MiB of HBM per device.

v0:
```python
import jax
import jax.numpy as jnp
from jax import lax
from jax.sharding import PartitionSpec as P

epsilon = 1e-06


def joined_along(parts, dim):
    shape = list(parts.shape[1:])
    shape[dim] *= parts.shape[0]
    return jnp.moveaxis(parts, 0, dim).reshape(shape)


def sent_to_all(shard, axis):
    length = lax.axis_size(axis)
    return lax.all_to_all(
        jnp.broadcast_to(shard[None], (length, *shard.shape)), axis, 0, 0, tiled=True
    )


def gathered_copies(shard, axis, dim):
    return joined_along(sent_to_all(shard, axis), dim)


def turned_gather(arrays, axis, dims):
    turned = [jnp.moveaxis(a, dim, 0) for a, dim in zip(arrays, dims)]
    widths = [t[0].size for t in turned]
    both = jnp.concatenate([t.reshape(-1, w) for t, w in zip(turned, widths)], axis=1)
    whole = lax.all_gather(both, axis, axis=0, tiled=True)
    parts = jnp.split(whole, [sum(widths[:k]) for k in range(1, len(widths))], axis=1)
    return tuple(
        (
            jnp.moveaxis(b.reshape(-1, *t.shape[1:]), 0, dim)
            for b, t, dim in zip(parts, turned, dims)
        )
    )


def in_blocks(shard, dim, length):
    before, after = (shard.shape[:dim], shard.shape[dim + 1 :])
    return jnp.moveaxis(shard.reshape(*before, length, -1, *after), dim, 0)


def summed_on_arrival(shard, axis, dim):
    parts = in_blocks(shard, dim, lax.axis_size(axis))
    arrived = lax.all_to_all(parts, axis, split_axis=0, concat_axis=0, tiled=True)
    return arrived.astype(jnp.float32).sum(axis=0)


def rms_rows(values, scaling):
    return values * lax.rsqrt(jnp.mean(values * values, axis=-1, keepdims=True) + epsilon) * scaling


def activate(lifted, up_scale):
    return jnp.square(jax.nn.relu(lifted * up_scale)).astype(jnp.bfloat16)


def on_device(tokens, pre_gain, up_weight, up_scale, down_weight, down_scale, post_gain):
    residual = tokens.astype(jnp.float32)
    normed = rms_rows(residual, pre_gain).astype(jnp.bfloat16)
    up_cast = up_weight.astype(jnp.bfloat16)
    down_cast = down_weight.astype(jnp.bfloat16)
    column_scales = gathered_copies(down_scale, "fs", 0)
    up_full, down_full = turned_gather((up_cast, down_cast), "fs", (0, 1))
    lifted = jnp.dot(normed, up_full, preferred_element_type=jnp.float32)
    hidden = activate(lifted, up_scale)
    partials = jnp.dot(hidden, down_full, preferred_element_type=jnp.float32)
    partials = (partials * column_scales).astype(jnp.bfloat16)
    summed = summed_on_arrival(partials, "tp", 0)
    branch = lax.optimization_barrier(summed.astype(jnp.bfloat16)).astype(jnp.float32)
    row_count = branch.shape[0]
    offset = lax.axis_index("tp") * row_count
    own_rows = lax.dynamic_slice_in_dim(residual, offset, row_count, 0)
    result = (own_rows + rms_rows(branch, post_gain)).astype(jnp.bfloat16)
    return gathered_copies(result, "tp", 0)


def solution(mesh):
    placed = (P(("grp", "fs"), None), P(), P("fs", "tp"), P("tp"), P("tp", "fs"), P("fs"), P())
    return jax.shard_map(
        on_device, mesh=mesh, in_specs=placed, out_specs=P(("grp", "fs"), None), check_vma=False
    )
```

profile of v0, /device:TPU:33, one launch (start us, length us, event | category | flops | bytes accessed | tf_op | source)
XLA Modules:
  0.0 268.8 jit_solution(17365989303714553077)
XLA Ops:
  6.5 0.0 all-gather.2.cloned.1.call-start
  6.6 1.0 convert_bitcast_fusion
  7.5 1.0 convert_element_type.28
  8.5 0.7 pad_maximum_fusion
  9.2 0.1 all-gather.2.cloned.1.call-update
  9.3 1.3 broadcast_in_dim.4
  10.5 46.3 %all-to-all-start = ((f32[32,1,64]{2,1,0:T(1,128)}), f32[32,1,64]{2,1,0:T(1,128)S(1)}, u32[]{:S(2)}, u32[]{:S(2)}) async-start(f32[32,1,64]{2,1,0:T(1,128)} %broadcast_in_dim.4), calls=%async_computation | async-start | bytes 32768 | tf_op jit(solution)/shard_map/all_to_all | solution.py:17
  56.8 2.1 multiply_reduce_fusion
  58.9 18.4 %all-to-all-done = f32[32,1,64]{2,1,0:T(1,128)S(1)} async-done(((f32[32,1,64]{2,1,0:T(1,128)}), f32[32,1,64]{2,1,0:T(1,128)S(1)}, u32[]{:S(2)}, u32[]{:S(2)}) %all-to-all-start) | async-done | bytes 8224 | tf_op jit(solution)/shard_map/all_to_all | solution.py:17
  77.4 0.5 broadcast.32
  77.9 0.6 reduce.4
  78.5 0.1 mul.67
  78.5 88.1 %all-gather.2.cloned.1.call-done = bf16[2048,2048]{1,0:T(8,128)(2,1)} async-done(((bf16[64,2048]{1,0:T(8,128)(2,1)}), bf16[2048,2048]{1,0:T(8,128)(2,1)}) %all-gather.2.cloned.1.call-update) | async-done | bytes 8388624 | tf_op jit(solution)/shard_map/all_gather | solution.py:30
  166.6 9.9 %multiply_convert_fusion = bf16[512,2048]{1,0:T(8,128)(2,1)} fusion(bf16[2048,2048]{1,0:T(8,128)(2,1)} %all-gather.2.cloned.1.call-done, f32[2048]{0:T(1024)S(1)} %mul.67, f32[2048]{0:T(1024)} %param.8, f32[512]{0:T(512)S(1)} %add_rsqrt_fusion, bf16[512,2048]{1,0:T(8,128)(2,1)} %param.7, f32[1024]{0:T(1024)} %param.10), kind=kOutput, calls=%fused_computation.4 | convolution fusion | flops 4303355904 | bytes 12605440 | tf_op jit(solution)/shard_map/dot_general | solution.py:68
  176.6 0.0 copy-start
  176.6 24.5 %all-to-all-start.1 = ((bf16[8,64,2048]{2,1,0:T(8,128)(2,1)}), bf16[8,64,2048]{2,1,0:T(8,128)(2,1)}, u32[]{:S(2)}, u32[]{:S(2)}) async-start(bf16[8,64,2048]{2,1,0:T(8,128)(2,1)} %bitcast.5), calls=%async_computation.1 | async-start | bytes 4194304 | tf_op jit(solution)/shard_map/all_to_all | solution.py:47
  201.1 0.0 copy-done
  201.1 0.0 copy-start.1
  201.1 2.5 convert_element_type.26
  203.5 23.9 %all-to-all-done.1 = bf16[8,64,2048]{2,1,0:T(8,128)(2,1)} async-done(((bf16[8,64,2048]{2,1,0:T(8,128)(2,1)}), bf16[8,64,2048]{2,1,0:T(8,128)(2,1)}, u32[]{:S(2)}, u32[]{:S(2)}) %all-to-all-start.1) | async-done | bytes 2097184 | tf_op jit(solution)/shard_map/all_to_all | solution.py:47
  227.4 2.0 reduce_sum.31
  229.3 0.2 fusion.15
  229.5 0.0 copy-done.1
  229.5 1.2 fusion.18
  230.7 0.2 broadcast_in_dim.5
  231.0 29.7 %all_to_all.16 = bf16[8,64,2048]{2,1,0:T(8,128)(2,1)S(1)} all-to-all(bf16[8,64,2048]{2,1,0:T(8,128)(2,1)S(1)} %broadcast_in_dim.5), channel_id=1, replica_groups=mesh['grp'=2,'fs'=32,'tp'=8] {'tp'}, dimensions={0} | all-to-all | bytes 4194304 | tf_op jit(solution)/shard_map/all_to_all | solution.py:17
  260.6 1.3 copy.9
  (2 shorter events, 0.0 us)
Async XLA Ops:
  6.5 160.1 %all-gather.2.cloned.1.call-start = ((), (), s32[]{:S(2)}) async-start(), calls=%async_computation.3 | async-start | bytes 8650752 | tf_op jit(solution)/shard_map/all_gather | solution.py:30
  10.5 66.8 %all-to-all-start = ((f32[32,1,64]{2,1,0:T(1,128)}), f32[32,1,64]{2,1,0:T(1,128)S(1)}, u32[]{:S(2)}, u32[]{:S(2)}) async-start(f32[32,1,64]{2,1,0:T(1,128)} %broadcast_in_dim.4), calls=%async_computation | async-start | bytes 32768 | tf_op jit(solution)/shard_map/all_to_all | solution.py:17
  176.6 24.5 %copy-start = (bf16[512,2048]{1,0:T(8,128)(2,1)S(1)}, bf16[512,2048]{1,0:T(8,128)(2,1)}, u32[]{:S(2)}) copy-start(bf16[512,2048]{1,0:T(8,128)(2,1)} %param.7) | copy-start | bytes 6291460
  176.6 50.8 %all-to-all-start.1 = ((bf16[8,64,2048]{2,1,0:T(8,128)(2,1)}), bf16[8,64,2048]{2,1,0:T(8,128)(2,1)}, u32[]{:S(2)}, u32[]{:S(2)}) async-start(bf16[8,64,2048]{2,1,0:T(8,128)(2,1)} %bitcast.5), calls=%async_computation.1 | async-start | bytes 4194304 | tf_op jit(solution)/shard_map/all_to_all | solution.py:47
  201.1 28.4 %copy-start.1 = (f32[2048]{0:T(1024)S(1)}, f32[2048]{0:T(1024)}, u32[]{:S(2)}) copy-start(f32[2048]{0:T(1024)} %param.13) | copy-start | bytes 24580
Sparse Core Ops, SparseCore 0:
  9.4 157.1 all-gather.1
where the time goes:
time: 269 us
  waiting for transfers between devices  130 us (48%)
  starting transfers between devices  70.8 us (26%)
  blocking collectives  29.7 us (11%)
  between operations  13.5 us (5%)
  other arithmetic  11.1 us (4%)
  matrix products  9.94 us (4%)
  local copies, waits for them, and re-layouts  3.39 us (1%)
    all_gather x1, waiting for transfers between devices, turned_gather(): whole = lax.all_gather(both, axis, axis=0, tiled=True)  88.1 us
    all_to_all x1, starting transfers between devices, sent_to_all(): lax.all_to_all(jnp.broadcast_to(shard[None], (length, *shard.shape)), axi...  46.3 us
    all_to_all x1, blocking collectives, sent_to_all(): lax.all_to_all(jnp.broadcast_to(shard[None], (length, *shard.shape)), axi...  29.7 us
    all_to_all x1, starting transfers between devices, summed_on_arrival(): lax.all_to_all(parts, axis, split_axis=0, concat_axis=0, tiled=True)  24.5 us
    all_to_all x1, waiting for transfers between devices, summed_on_arrival(): lax.all_to_all(parts, axis, split_axis=0, concat_axis=0, tiled=True)  23.9 us
    all_to_all x1, waiting for transfers between devices, sent_to_all(): lax.all_to_all(jnp.broadcast_to(shard[None], (length, *shard.shape)), axi...  18.4 us
    dot_general x1, matrix products, on_device(): partials = jnp.dot(hidden, down_full, preferred_element_type=jnp.float32)  9.94 us
  transfers between devices with their start and end apart: 3, of which 3 were waited for; matrix products, arithmetic and copies ran while one was open for 3% of the time, Pallas kernels for 0%

commit v1 on v0

v1 whole, which is shorter than its diff:
```python
import functools

import jax
import jax.numpy as jnp
from jax import lax
from jax.experimental import pallas as pl
from jax.experimental.pallas import tpu as pltpu
from jax.sharding import PartitionSpec as P

epsilon = 1e-06
MESH = pl.DeviceIdType.MESH

LAG = 8
PER = 2
UP_PARTS = 2
TOKEN_PARTS = 4


def remote(src, dst, send_sem, recv_sem, **where):
    return pltpu.make_async_remote_copy(
        src_ref=src, dst_ref=dst, send_sem=send_sem, recv_sem=recv_sem, device_id=where, device_id_type=MESH
    )


def arrived(ref, sem):
    pltpu.make_async_copy(ref, ref, sem).wait()


def kernel(
    nz, nx, tok, gain, upb, dnb, post, out,
    up, down, other, normed, acc, hidden, part, ypart, xpart, branch,
    up_in, down_in, up_sib, down_sib, tok_in, y_in, x_in, all_in, branch_sib,
    up_out, down_out, up_sib_out, down_sib_out, tok_out, y_out, x_out, all_out, all_sib_out,
):
    half = nz // 2
    rows, width = tok.shape
    block = width // nz
    quad = 4 * block
    n_quads = width // quad
    own = rows // nx
    tok_rows = rows // TOKEN_PARTS

    g = lax.axis_index("grp")
    z = lax.axis_index("fs")
    t = lax.axis_index("tp")
    y = lax.rem(g, 2)
    c = lax.rem(t, 2)
    x = t // 2
    partner = g + 1 - 2 * y
    sibling = t + 1 - 2 * c
    right = lax.rem(z + 1, nz)
    left = lax.rem(z + nz - 1, nz)
    home = c == y
    z_quad = z // 4

    def peer(i):
        return lax.rem(x + i, nx)

    barrier = pltpu.get_barrier_semaphore()
    neighbours = [{"fs": left}, {"fs": right}, {"tp": sibling}, {"grp": partner}]
    neighbours += [{"tp": 2 * peer(i) + c} for i in range(1, nx)]
    for where in neighbours:
        pl.semaphore_signal(barrier, inc=1, device_id=where, device_id_type=MESH)
    pl.semaphore_wait(barrier, len(neighbours))

    def quad_of(j):
        step = (j + 1) // 2
        return lax.rem(z_quad + n_quads + jnp.where(lax.rem(j, 2) == 1, -step, step), n_quads)

    def at_block(buf, b, k=0, parts=1):
        piece = block // parts
        return buf.at[c, pl.ds(pl.multiple_of(b * block + k * piece, piece), piece)]

    def begin(src, buf, in_sem, sib_sem, out_sem, sib_out, parts):
        piece = block // parts
        for k in range(parts):
            view = src.at[pl.ds(k * piece, piece)]
            for there in (right, left):
                remote(view, at_block(buf, z, k, parts), out_sem, in_sem.at[z * parts + k], fs=there).start()
        remote(src, at_block(buf, z), sib_out, sib_sem.at[0], tp=sibling).start()

    def ring_step(s, buf, in_sem, sib_sem, out_sem, sib_out, parts):
        back = lax.rem(z + nz - s, nz)
        ahead = lax.rem(z + s, nz)
        for k in range(parts):
            view = at_block(buf, back, k, parts)
            sem = in_sem.at[back * parts + k]
            arrived(view, sem)

            @pl.when(s < half)
            def _():
                remote(view, view, out_sem, sem, fs=right).start()

            @pl.when(s < half)
            def _():
                view = at_block(buf, ahead, k, parts)
                sem = in_sem.at[ahead * parts + k]
                arrived(view, sem)

                @pl.when(s < half - 1)
                def _():
                    remote(view, view, out_sem, sem, fs=left).start()

        view = at_block(buf, back)
        remote(view, view, sib_out, sib_sem.at[s // 4], tp=sibling).start()

        @pl.when(s < half)
        def _():
            view = at_block(buf, ahead)
            remote(view, view, sib_out, sib_sem.at[s // 4], tp=sibling).start()

    def from_sibling(j, buf, sib_sem):
        @pl.when(j == 0)
        def _():
            arrived(buf.at[1 - c, pl.ds(0, 7 * block)], sib_sem.at[0])

        @pl.when((lax.rem(j, 2) == 1) & (j < n_quads - 1))
        def _():
            arrived(buf.at[1 - c, pl.ds(0, 8 * block)], sib_sem.at[(j + 1) // 2])

        @pl.when(j == n_quads - 1)
        def _():
            arrived(buf.at[1 - c, pl.ds(0, block)], sib_sem.at[n_quads // 2])

    up_args = (up, up_in, up_sib, up_out, up_sib_out, UP_PARTS)
    down_args = (down, down_in, down_sib, down_out, down_sib_out, 1)
    begin(upb, *up_args)

    @pl.when(home)
    def _():
        for k in range(TOKEN_PARTS):
            view = pl.ds(k * tok_rows, tok_rows)
            remote(tok.at[view], other.at[view], tok_out, tok_in.at[k], grp=partner).start()

    begin(dnb, *down_args)
    up[c, pl.ds(pl.multiple_of(z * block, block), block), :] = upb[...]
    down[c, pl.ds(pl.multiple_of(z * block, block), block), :] = dnb[...]
    acc[...] = jnp.zeros_like(acc)

    def normalize(k):
        step = 32

        def from_rows(src):
            def body(i, _):
                view = pl.ds(pl.multiple_of(k * tok_rows + i * step, step), step)
                values = src[view, :].astype(jnp.float32)
                mean = jnp.mean(values * values, axis=-1, keepdims=True)
                scaled = (values * lax.rsqrt(mean + epsilon) * gain[...]).astype(jnp.bfloat16)
                for q in range(n_quads):
                    normed[q, view, :] = scaled[:, q * quad : (q + 1) * quad]
                return 0

            lax.fori_loop(0, tok_rows // step, body, 0)

        @pl.when(home)
        def _():
            from_rows(tok)

        @pl.when(jnp.logical_not(home))
        def _():
            view = pl.ds(pl.multiple_of(k * tok_rows, tok_rows), tok_rows)
            arrived(other.at[view], tok_in.at[k])
            from_rows(other)

    def lift(j):
        from_sibling(j, up, up_sib)
        q = quad_of(j)
        view = pl.ds(pl.multiple_of(q * quad, quad), quad)
        for h in range(2):
            acc[h] += jnp.dot(normed[q], up[h, view, :], preferred_element_type=jnp.float32)

    first = 10

    def up_pass(s, _):
        ring_step(s, *up_args)

        @pl.when(s > LAG)
        def _():
            ring_step(s - LAG, *down_args)

        @pl.when((lax.rem(s, 2) == 1) & (s >= 3) & (s < 3 + 2 * TOKEN_PARTS))
        def _():
            normalize((s - 3) // 2)

        @pl.when((s >= first) & (s < half))
        def _():
            lift(s - first)

        return 0

    lax.fori_loop(1, half + 1, up_pass, 0)

    def lift_rest(j, _):
        lift(j)
        return 0

    lax.fori_loop(half - first, n_quads, lift_rest, 0)
    for h in range(2):
        hidden[h] = jnp.square(jnp.maximum(acc[h], 0.0)).astype(jnp.bfloat16)

    own_rows = pl.ds(pl.multiple_of(x * own, own), own)

    def project(j):
        from_sibling(j, down, down_sib)
        q = quad_of(j)
        view = pl.ds(pl.multiple_of(q * quad, quad), quad)
        total = None
        for h in range(2):
            term = lax.dot_general(
                hidden[h], down[h, view, :], (((1,), (1,)), ((), ())), preferred_element_type=jnp.float32
            )
            total = term if total is None else total + term
        part[j] = total.astype(jnp.bfloat16)

        @pl.when(jnp.logical_not(home))
        def _():
            remote(part.at[j], ypart.at[j], y_out, y_in.at[j], grp=partner).start()

    def pair_sum(j):
        arrived(ypart.at[j], y_in.at[j])
        part[j] = (part[j].astype(jnp.float32) + ypart[j].astype(jnp.float32)).astype(jnp.bfloat16)
        for i in range(1, nx):
            view = pl.ds(pl.multiple_of(peer(i) * own, own), own)
            slot = nx - 1 - i
            remote(
                part.at[j, view], xpart.at[slot, j], x_out, x_in.at[slot * n_quads + j], tp=2 * peer(i) + c
            ).start()

    def row_sum(j):
        q = quad_of(j)
        total = part[j, own_rows, :].astype(jnp.float32)
        for i in range(nx - 1):
            arrived(xpart.at[i, j], x_in.at[i * n_quads + j])
            total += xpart[i, j].astype(jnp.float32)
        branch[q, own_rows, :] = total.astype(jnp.bfloat16)
        view = branch.at[q, own_rows]
        for i in range(1, nx):
            slot = nx - 1 - i
            remote(view, view, all_out, all_in.at[slot * n_quads + j], tp=2 * peer(i) + c).start()
        remote(view, view, all_sib_out, branch_sib, tp=sibling).start()

    def hand_on(j):
        q = quad_of(j)
        for i in range(1, nx):
            view = branch.at[q, pl.ds(pl.multiple_of(peer(i) * own, own), own)]
            arrived(view, all_in.at[(i - 1) * n_quads + j])
            remote(view, view, all_sib_out, branch_sib, tp=sibling).start()

    def output_pass(i, _):
        done = half - LAG + PER * i

        def more(s, _):
            ring_step(s, *down_args)
            return 0

        lax.fori_loop(jnp.minimum(done, half) + 1, jnp.minimum(done + PER, half) + 1, more, 0)

        @pl.when(i < n_quads)
        def _():
            project(i)

        @pl.when(home)
        def _():
            for behind, stage in ((1, pair_sum), (2, row_sum), (3, hand_on)):

                @pl.when((i >= behind) & (i < n_quads + behind))
                def _():
                    stage(i - behind)

        return 0

    lax.fori_loop(0, n_quads + 3, output_pass, 0)

    sent = (nz - 1) * block
    for buf, out_sem, sib_out in ((up, up_out, up_sib_out), (down, down_out, down_sib_out)):
        arrived(buf.at[0, pl.ds(0, sent)], out_sem)
        arrived(buf.at[0], sib_out)

    @pl.when(home)
    def _():
        arrived(tok, tok_out)
        most = part.at[pl.ds(0, n_quads * (nx - 1) // nx)]
        arrived(most, x_out)
        arrived(most, all_out)
        arrived(part, all_sib_out)

    @pl.when(jnp.logical_not(home))
    def _():
        arrived(part, y_out)
        arrived(branch, branch_sib)

    step = 32

    def finish(i, _):
        view = pl.ds(pl.multiple_of(i * step, step), step)
        squares = jnp.zeros((step, 1), jnp.float32)
        for q in range(n_quads):
            values = branch[q, view, :].astype(jnp.float32)
            squares += jnp.sum(values * values, axis=-1, keepdims=True)
        scale = lax.rsqrt(squares / width + epsilon)
        for q in range(n_quads):
            cols = slice(q * quad, (q + 1) * quad)
            values = branch[q, view, :].astype(jnp.float32)
            result = tok[view, cols].astype(jnp.float32) + values * scale * post[:, cols]
            out[view, cols] = result.astype(jnp.bfloat16)
        return 0

    lax.fori_loop(0, rows // step, finish, 0)


def solution(mesh):
    nz, nx = mesh.shape["fs"], mesh.shape["tp"] // 2

    def on_device(tokens, pre_gain, up_weight, up_scale, down_weight, down_scale, post_gain):
        rows, width = tokens.shape
        block, units = up_weight.shape
        mine = units // 2
        offset = lax.rem(lax.axis_index("grp"), 2) * mine
        upb = lax.dynamic_slice_in_dim(up_weight * up_scale, offset, mine, 1).astype(jnp.bfloat16)
        dnb = lax.dynamic_slice_in_dim(down_weight, offset, mine, 0) * down_scale
        dnb = dnb.T.astype(jnp.bfloat16)
        quad = 4 * block
        n_quads = width // quad
        own = rows // nx
        vmem = pl.BlockSpec(memory_space=pltpu.VMEM)
        bf16, f32 = jnp.bfloat16, jnp.float32
        dma = pltpu.SemaphoreType.DMA
        return pl.pallas_call(
            functools.partial(kernel, nz, nx),
            out_shape=jax.ShapeDtypeStruct((rows, width), bf16),
            in_specs=[vmem] * 5,
            out_specs=vmem,
            scratch_shapes=[
                pltpu.VMEM((2, width, mine), bf16),
                pltpu.VMEM((2, width, mine), bf16),
                pltpu.VMEM((rows, width), bf16),
                pltpu.VMEM((n_quads, rows, quad), bf16),
                pltpu.VMEM((2, rows, mine), f32),
                pltpu.VMEM((2, rows, mine), bf16),
                pltpu.VMEM((n_quads, rows, quad), bf16),
                pltpu.VMEM((n_quads, rows, quad), bf16),
                pltpu.VMEM((nx - 1, n_quads, own, quad), bf16),
                pltpu.VMEM((n_quads, rows, quad), bf16),
                dma((nz * UP_PARTS,)),
                dma((nz,)),
                dma((nz // 8 + 1,)),
                dma((nz // 8 + 1,)),
                dma((TOKEN_PARTS,)),
                dma((n_quads,)),
                dma(((nx - 1) * n_quads,)),
                dma(((nx - 1) * n_quads,)),
                dma,
                dma,
                dma,
                dma,
                dma,
                dma,
                dma,
                dma,
                dma,
                dma,
            ],
            compiler_params=pltpu.CompilerParams(
                collective_id=0, has_side_effects=True, vmem_limit_bytes=60 * 1024 * 1024
            ),
        )(tokens, pre_gain.reshape(1, width), upb, dnb, post_gain.reshape(1, width))

    placed = (P(("grp", "fs"), None), P(), P("fs", "tp"), P("tp"), P("tp", "fs"), P("fs"), P())
    return jax.shard_map(
        on_device, mesh=mesh, in_specs=placed, out_specs=P(("grp", "fs"), None), check_vma=False
    )
```

time: 269 us -> 176 us (0.65)
  Pallas kernels: 0 us -> 169 us
  waiting for transfers between devices: 130 us -> 0 us
  starting transfers between devices: 70.8 us -> 0 us
  blocking collectives: 29.7 us -> 0 us
  between operations: 13.5 us -> 0.01 us
  matrix products: 9.94 us -> 0 us
  other arithmetic: 11.1 us -> 3.15 us
    pallas_call x0 -> x1, Pallas kernels: none -> 169 us  [on_device(): pl.pallas_call(functools.partial(kernel, nz, nx), out_shape=jax.ShapeDtyp...]
    all_gather x1 -> x0, waiting for transfers between devices: 88.1 us -> none  [turned_gather(): whole = lax.all_gather(both, axis, axis=0, tiled=True)]
    all_to_all x2 -> x0, starting transfers between devices: 70.8 us -> none  [the longest x1 46.3 us: sent_to_all(): lax.all_to_all(jnp.broadcast_to(shard[None], (length, *shard.shape)), axi...]
    all_to_all x2 -> x0, waiting for transfers between devices: 42.3 us -> none  [the longest x1 23.9 us: summed_on_arrival(): lax.all_to_all(parts, axis, split_axis=0, concat_axis=0, tiled=True)]
    all_to_all x1 -> x0, blocking collectives: 29.7 us -> none  [sent_to_all(): lax.all_to_all(jnp.broadcast_to(shard[None], (length, *shard.shape)), axi...]
    dot_general x1 -> x0, matrix products: 9.94 us -> none  [on_device(): partials = jnp.dot(hidden, down_full, preferred_element_type=jnp.float32)]
    reduce_sum x3 -> x0, other arithmetic: 4.19 us -> none  [the longest x2 2.23 us: rms_rows(): jnp.mean(values * values, axis=-1, keepdims=True) + epsilon]
  transfers between devices with their start and end apart: 3 -> 0, of which waited for: 3 -> 0; matrix products, arithmetic and copies ran while one was open for 3% -> 0% of each run, Pallas kernels for 0% -> 0%
where the time goes in v1:
time: 176 us
  Pallas kernels  169 us (96%)
  local copies, waits for them, and re-layouts  3.92 us (2%)
  other arithmetic  3.15 us (2%)
    pallas_call x1, Pallas kernels, on_device(): pl.pallas_call(functools.partial(kernel, nz, nx), out_shape=jax.ShapeDtyp...  169 us

profile of v1, /device:TPU:33, one launch (start us, length us, event | category | flops | bytes accessed | tf_op | source)
XLA Modules:
  0.0 175.8 jit_solution(15681134580043698063)
XLA Ops:
  0.0 0.8 dynamic-slice
  0.8 1.5 fusion.upb
  2.3 1.6 fusion.1.dnb
  3.9 168.7 %shard_map.73 = bf16[512,2048]{1,0:T(8,128)(2,1)} custom-call(bf16[512,2048]{1,0:T(8,128)(2,1)} %tok.1, f32[1,2048]{1,0:T(1,128)} %bitcast.4, bf16[64,512]{1,0:T(8,128)(2,1)} %fusion.upb, bf16[64,512]{1,0:T(8,128)(2,1)} %fusion.1.dnb, f32[1,2048]{1,0:T(1,128)} %bitcast.5), custom_call_target="tpu_custom_call" | custom-call | tf_op jit(solution)/shard_map/pallas_call | solution.py:328
  172.6 3.2 %copy.9 = bf16[512,2048]{1,0:T(8,128)(2,1)} copy(bf16[512,2048]{1,0:T(8,128)(2,1)} %shard_map.73) | data formatting | bytes 4194304

commit v2 on v1

v2 whole, which is shorter than its diff:
```python
import functools

import jax
import jax.numpy as jnp
from jax import lax
from jax.experimental import pallas as pl
from jax.experimental.pallas import tpu as pltpu
from jax.sharding import PartitionSpec as P

epsilon = 1e-06
MESH = pl.DeviceIdType.MESH

LAG = 6
PER = 2
PARTS = 2
TOKEN_PARTS = 4
ORDER = (1, 2, 0, 3, 7, 4, 6, 5)


def remote(src, dst, send_sem, recv_sem, **where):
    return pltpu.make_async_remote_copy(
        src_ref=src, dst_ref=dst, send_sem=send_sem, recv_sem=recv_sem, device_id=where, device_id_type=MESH
    )


def arrived(ref, sem):
    pltpu.make_async_copy(ref, ref, sem).wait()


def kernel(
    nz, nx, tok, gain, up_w, up_s, down_w, down_s, post, out,
    up, down, other, normed, acc, hidden, part, ypart, xpart, branch,
    up_in, down_in, up_sib, down_sib, tok_in, y_in, x_in, all_in, branch_sib,
    up_out, down_out, up_sib_out, down_sib_out, own_sib_out, tok_out, y_out, x_out, all_out, all_sib_out,
):
    rows, width = tok.shape
    block, units = up_w.shape
    mine = units // 2
    quad = 4 * block
    n_quads = width // quad
    own = rows // nx
    tok_rows = rows // TOKEN_PARTS
    piece = block // PARTS
    reach = (nz * 13 // 32, nz - 1 - nz * 13 // 32)

    g = lax.axis_index("grp")
    z = lax.axis_index("fs")
    t = lax.axis_index("tp")
    y = lax.rem(g, 2)
    c = lax.rem(t, 2)
    x = t // 2
    partner = g + 1 - 2 * y
    sibling = t + 1 - 2 * c
    way = 1 - 2 * c
    following = lax.rem(z + way + nz, nz)
    previous = lax.rem(z - way + nz, nz)
    home = c == y
    z_quad = z // 4
    last = jnp.where(c == 0, reach[0], reach[1])

    def peer(i):
        return lax.rem(x + i, nx)

    barrier = pltpu.get_barrier_semaphore()
    neighbours = [{"fs": previous}, {"tp": sibling}, {"grp": partner}]
    neighbours += [{"tp": 2 * peer(i) + c} for i in range(1, nx)]
    for where in neighbours:
        pl.semaphore_signal(barrier, inc=1, device_id=where, device_id_type=MESH)

    half = pl.ds(pl.multiple_of(y * mine, mine), mine)
    up[z, c] = (up_w[:, half] * up_s[:, half]).astype(jnp.bfloat16)
    line = lax.broadcasted_iota(jnp.int32, (block, block), 0) == lax.broadcasted_iota(jnp.int32, (block, block), 1)
    column = jnp.sum(jnp.where(line, jnp.broadcast_to(down_s[...], (block, block)), 0.0), axis=1, keepdims=True)
    down[z, c] = (down_w[:, half] * column).astype(jnp.bfloat16)
    acc[...] = jnp.zeros_like(acc)
    pl.semaphore_wait(barrier, len(neighbours))

    def quad_of(j):
        return lax.rem(z_quad + sum(jnp.where(j == k, ORDER[k], 0) for k in range(n_quads)), n_quads)

    def send_half(b, h, buf, in_sem, out_sem, wait):
        for k in range(PARTS):
            view = buf.at[b, h, pl.ds(k * piece, piece)]
            sem = in_sem.at[(2 * b + h) * PARTS + k]
            if wait is not None:
                arrived(view, sem)

            @pl.when(True if wait is None else wait)
            def _():
                remote(view, view, out_sem, sem, fs=following).start()

    def begin(buf, in_sem, sib_sem, out_sem, sib_out):
        send_half(z, c, buf, in_sem, out_sem, None)
        arrived(buf.at[z, 1 - c], sib_sem.at[z])
        send_half(z, 1 - c, buf, in_sem, out_sem, None)

    def ring_step(s, buf, in_sem, sib_sem, out_sem, sib_out):
        b = lax.rem(z - way * s + nz, nz)
        for h in (c, 1 - c):
            send_half(b, h, buf, in_sem, out_sem, s < last)
        remote(buf.at[b], buf.at[b], sib_out, sib_sem.at[b], tp=sibling).start()

    def from_sibling(q, buf, sib_sem):
        for i in range(4):
            b = 4 * q + i
            ahead = lax.rem(b - z + nz, nz)

            @pl.when((ahead > 0) & jnp.where(c == 0, ahead <= reach[1], ahead > reach[1]))
            def _():
                arrived(buf.at[b], sib_sem.at[b])

    up_args = (up, up_in, up_sib, up_out, up_sib_out)
    down_args = (down, down_in, down_sib, down_out, down_sib_out)
    for buf, sib_sem in ((up, up_sib), (down, down_sib)):
        remote(buf.at[z, c], buf.at[z, c], own_sib_out, sib_sem.at[z], tp=sibling).start()
    begin(*up_args)

    @pl.when(home)
    def _():
        for k in range(TOKEN_PARTS):
            view = pl.ds(k * tok_rows, tok_rows)
            remote(tok.at[view], other.at[view], tok_out, tok_in.at[k], grp=partner).start()

    def normalize(k):
        step = 32

        def from_rows(src):
            def body(i, _):
                view = pl.ds(pl.multiple_of(k * tok_rows + i * step, step), step)
                values = src[view, :].astype(jnp.float32)
                mean = jnp.mean(values * values, axis=-1, keepdims=True)
                scaled = (values * lax.rsqrt(mean + epsilon) * gain[...]).astype(jnp.bfloat16)
                for q in range(n_quads):
                    normed[q, view, :] = scaled[:, q * quad : (q + 1) * quad]
                return 0

            lax.fori_loop(0, tok_rows // step, body, 0)

        @pl.when(home)
        def _():
            from_rows(tok)

        @pl.when(jnp.logical_not(home))
        def _():
            view = pl.ds(pl.multiple_of(k * tok_rows, tok_rows), tok_rows)
            arrived(other.at[view], tok_in.at[k])
            from_rows(other)

    def lift(m):
        q = lax.rem(z_quad - way * m + n_quads + 8, n_quads)
        from_sibling(q, up, up_sib)
        for h in range(2):
            weights = up[pl.ds(4 * q, 4), h].reshape(quad, mine)
            acc[h] += jnp.dot(normed[q], weights, preferred_element_type=jnp.float32)

    norm_at = 8
    lift_at = norm_at + TOKEN_PARTS

    def up_pass(s, _):
        ring_step(s, *up_args)

        @pl.when(s == LAG)
        def _():
            begin(*down_args)

        @pl.when(s > LAG)
        def _():
            ring_step(s - LAG, *down_args)

        @pl.when((s >= norm_at) & (s < lift_at))
        def _():
            normalize(s - norm_at)

        @pl.when((s == lift_at) | (s == lift_at + 1) | (s == lift_at + 4))
        def _():
            lift(jnp.minimum(s - lift_at + 1, 3))

        return 0

    lax.fori_loop(1, last + 1, up_pass, 0)

    def lift_rest(m, _):
        lift(m)
        return 0

    lax.fori_loop(jnp.where(c == 0, 3, 4), n_quads + 1, lift_rest, 0)
    for h in range(2):
        hidden[h] = jnp.square(jnp.maximum(acc[h], 0.0)).astype(jnp.bfloat16)

    own_rows = pl.ds(pl.multiple_of(x * own, own), own)

    def project(j):
        q = quad_of(j)
        from_sibling(q, down, down_sib)
        total = None
        for h in range(2):
            weights = down[pl.ds(4 * q, 4), h].reshape(quad, mine)
            term = lax.dot_general(
                hidden[h], weights, (((1,), (1,)), ((), ())), preferred_element_type=jnp.float32
            )
            total = term if total is None else total + term
        part[j] = total.astype(jnp.bfloat16)

        @pl.when(jnp.logical_not(home))
        def _():
            remote(part.at[j], ypart.at[j], y_out, y_in.at[j], grp=partner).start()

    def pair_sum(j):
        arrived(ypart.at[j], y_in.at[j])
        part[j] = (part[j].astype(jnp.float32) + ypart[j].astype(jnp.float32)).astype(jnp.bfloat16)
        for i in range(1, nx):
            view = pl.ds(pl.multiple_of(peer(i) * own, own), own)
            slot = nx - 1 - i
            remote(
                part.at[j, view], xpart.at[slot, j], x_out, x_in.at[slot * n_quads + j], tp=2 * peer(i) + c
            ).start()

    def row_sum(j):
        q = quad_of(j)
        total = part[j, own_rows, :].astype(jnp.float32)
        for i in range(nx - 1):
            arrived(xpart.at[i, j], x_in.at[i * n_quads + j])
            total += xpart[i, j].astype(jnp.float32)
        branch[q, own_rows, :] = total.astype(jnp.bfloat16)
        view = branch.at[q, own_rows]
        for i in (1, nx - 1):
            remote(view, view, all_out, all_in.at[(nx - 1 - i) * n_quads + j], tp=2 * peer(i) + c).start()
        remote(view, view, all_sib_out, branch_sib, tp=sibling).start()

    def take(i, j):
        view = branch.at[quad_of(j), pl.ds(pl.multiple_of(peer(i) * own, own), own)]
        arrived(view, all_in.at[(i - 1) * n_quads + j])
        remote(view, view, all_sib_out, branch_sib, tp=sibling).start()
        return view

    def hand_on(j):
        view = take(1, j)
        remote(view, view, all_out, all_in.at[n_quads + j], tp=2 * peer(nx - 1) + c).start()
        take(nx - 1, j)

    def hand_far(j):
        take(2, j)

    def output_pass(i, _):
        done = last - LAG + PER * i

        def more(s, _):
            ring_step(s, *down_args)
            return 0

        lax.fori_loop(jnp.minimum(done, last) + 1, jnp.minimum(done + PER, last) + 1, more, 0)

        @pl.when(i < n_quads)
        def _():
            project(i)

        @pl.when(home)
        def _():
            for behind, stage in ((1, pair_sum), (2, row_sum), (3, hand_on), (4, hand_far)):

                @pl.when((i >= behind) & (i < n_quads + behind))
                def _():
                    stage(i - behind)

        return 0

    lax.fori_loop(0, n_quads + 4, output_pass, 0)

    for side in range(2):

        @pl.when(c == side)
        def _():
            for sem in (up_out, down_out, up_sib_out, down_sib_out):
                arrived(up.at[pl.ds(0, reach[side])], sem)

    arrived(up.at[0], own_sib_out)

    @pl.when(home)
    def _():
        arrived(tok, tok_out)
        most = part.at[pl.ds(0, n_quads * (nx - 1) // nx)]
        arrived(most, x_out)
        arrived(most, all_out)
        arrived(part, all_sib_out)

    @pl.when(jnp.logical_not(home))
    def _():
        arrived(part, y_out)
        arrived(branch, branch_sib)

    step = 32

    def finish(i, _):
        view = pl.ds(pl.multiple_of(i * step, step), step)
        squares = jnp.zeros((step, 1), jnp.float32)
        for q in range(n_quads):
            values = branch[q, view, :].astype(jnp.float32)
            squares += jnp.sum(values * values, axis=-1, keepdims=True)
        scale = lax.rsqrt(squares / width + epsilon)
        for q in range(n_quads):
            cols = slice(q * quad, (q + 1) * quad)
            values = branch[q, view, :].astype(jnp.float32)
            result = tok[view, cols].astype(jnp.float32) + values * scale * post[:, cols]
            out[view, cols] = result.astype(jnp.bfloat16)
        return 0

    lax.fori_loop(0, rows // step, finish, 0)


def solution(mesh):
    nz, nx = mesh.shape["fs"], mesh.shape["tp"] // 2

    def on_device(tokens, pre_gain, up_weight, up_scale, down_weight, down_scale, post_gain):
        rows, width = tokens.shape
        block, units = up_weight.shape
        mine = units // 2
        quad = 4 * block
        n_quads = width // quad
        own = rows // nx
        vmem = pl.BlockSpec(memory_space=pltpu.VMEM)
        bf16, f32 = jnp.bfloat16, jnp.float32
        dma = pltpu.SemaphoreType.DMA
        return pl.pallas_call(
            functools.partial(kernel, nz, nx),
            out_shape=jax.ShapeDtypeStruct((rows, width), bf16),
            in_specs=[vmem] * 7,
            out_specs=vmem,
            scratch_shapes=[
                pltpu.VMEM((nz, 2, block, mine), bf16),
                pltpu.VMEM((nz, 2, block, mine), bf16),
                pltpu.VMEM((rows, width), bf16),
                pltpu.VMEM((n_quads, rows, quad), bf16),
                pltpu.VMEM((2, rows, mine), f32),
                pltpu.VMEM((2, rows, mine), bf16),
                pltpu.VMEM((n_quads, rows, quad), bf16),
                pltpu.VMEM((n_quads, rows, quad), bf16),
                pltpu.VMEM((nx - 1, n_quads, own, quad), bf16),
                pltpu.VMEM((n_quads, rows, quad), bf16),
                dma((nz * 2 * PARTS,)),
                dma((nz * 2 * PARTS,)),
                dma((nz,)),
                dma((nz,)),
                dma((TOKEN_PARTS,)),
                dma((n_quads,)),
                dma(((nx - 1) * n_quads,)),
                dma(((nx - 1) * n_quads,)),
                dma,
                dma,
                dma,
                dma,
                dma,
                dma,
                dma,
                dma,
                dma,
                dma,
                dma,
            ],
            compiler_params=pltpu.CompilerParams(
                collective_id=0, has_side_effects=True, vmem_limit_bytes=60 * 1024 * 1024
            ),
        )(
            tokens,
            pre_gain.reshape(1, width),
            up_weight,
            up_scale.reshape(1, units),
            down_weight.T,
            down_scale.reshape(1, block),
            post_gain.reshape(1, width),
        )

    placed = (P(("grp", "fs"), None), P(), P("fs", "tp"), P("tp"), P("tp", "fs"), P("fs"), P())
    return jax.shard_map(
        on_device, mesh=mesh, in_specs=placed, out_specs=P(("grp", "fs"), None), check_vma=False
    )
```

time: 176 us -> 161 us (0.915)
  Pallas kernels: 169 us -> 158 us
  other arithmetic: 3.15 us -> 0 us
    pallas_call x1, Pallas kernels: 169 us -> 158 us  [on_device(): pl.pallas_call(functools.partial(kernel, nz, nx), out_shape=jax.ShapeDtyp...]
    convert_element_type x2 -> x0, other arithmetic: 3.15 us -> none  [the longest x1 1.6 us: on_device(): dnb = dnb.T.astype(jnp.bfloat16)]
where the time goes in v2:
time: 161 us
  Pallas kernels  158 us (98%)
  local copies, waits for them, and re-layouts  3.16 us (2%)
    pallas_call x1, Pallas kernels, on_device(): pl.pallas_call(functools.partial(kernel, nz, nx), out_shape=jax.ShapeDtyp...  158 us

profile of v2, /device:TPU:33, one launch (start us, length us, event | category | flops | bytes accessed | tf_op | source)
XLA Modules:
  0.0 161.1 jit_solution(12438167840378778845)
XLA Ops:
  0.0 158.0 %shard_map.73 = bf16[512,2048]{1,0:T(8,128)(2,1)} custom-call(bf16[512,2048]{1,0:T(8,128)(2,1)} %tok.1, f32[1,2048]{1,0:T(1,128)} %bitcast.6, f32[64,1024]{1,0:T(8,128)} %up_w.1, f32[1,1024]{1,0:T(1,128)} %bitcast.8, f32[64,1024]{1,0:T(8,128)} %bitcast.5, f32[1,64]{1,0:T(1,128)} %bitcast.9, f32[1,2048]{1,0:T(1,128)} %bitcast.7), custom_call_target="tpu_custom_call" | custom-call | tf_op jit(solution)/shard_map/pallas_call | solution.py:323
  158.0 3.2 %copy.9 = bf16[512,2048]{1,0:T(8,128)(2,1)} copy(bf16[512,2048]{1,0:T(8,128)(2,1)} %shard_map.73) | data formatting | bytes 4194304

commit v3 on v2

--- a/solution.py
+++ b/solution.py
@@ -10,8 +10,7 @@
 epsilon = 1e-06
 MESH = pl.DeviceIdType.MESH
 
-LAG = 6
-PER = 2
+LAG = 2
 PARTS = 2
 TOKEN_PARTS = 4
 ORDER = (1, 2, 0, 3, 7, 4, 6, 5)
@@ -28,10 +27,10 @@
 
 
 def kernel(
-    nz, nx, tok, gain, up_w, up_s, down_w, down_s, post, out,
-    up, down, other, normed, acc, hidden, part, ypart, xpart, branch,
+    nz, nx, tok, gain, up_w, up_s, down_w, down_s, out,
+    up, down, seen, normed, acc, hidden, part, ypart, xpart, branch,
     up_in, down_in, up_sib, down_sib, tok_in, y_in, x_in, all_in, branch_sib,
-    up_out, down_out, up_sib_out, down_sib_out, own_sib_out, tok_out, y_out, x_out, all_out, all_sib_out,
+    up_out, down_out, up_sib_out, down_sib_out, own_sib_out, tok_out, y_out, x_out, all_out, all_sib_out, out_sem,
 ):
     rows, width = tok.shape
     block, units = up_w.shape
@@ -67,12 +66,19 @@
     for where in neighbours:
         pl.semaphore_signal(barrier, inc=1, device_id=where, device_id_type=MESH)
 
+    def token_rows(k):
+        return pl.ds(pl.multiple_of(k * tok_rows, tok_rows), tok_rows)
+
+    @pl.when(home)
+    def _():
+        for k in range(TOKEN_PARTS):
+            pltpu.make_async_copy(tok.at[token_rows(k)], seen.at[token_rows(k)], tok_in.at[k]).start()
+
     half = pl.ds(pl.multiple_of(y * mine, mine), mine)
     up[z, c] = (up_w[:, half] * up_s[:, half]).astype(jnp.bfloat16)
     line = lax.broadcasted_iota(jnp.int32, (block, block), 0) == lax.broadcasted_iota(jnp.int32, (block, block), 1)
     column = jnp.sum(jnp.where(line, jnp.broadcast_to(down_s[...], (block, block)), 0.0), axis=1, keepdims=True)
     down[z, c] = (down_w[:, half] * column).astype(jnp.bfloat16)
-    acc[...] = jnp.zeros_like(acc)
     pl.semaphore_wait(barrier, len(neighbours))
 
     def quad_of(j):
@@ -113,38 +119,29 @@
     down_args = (down, down_in, down_sib, down_out, down_sib_out)
     for buf, sib_sem in ((up, up_sib), (down, down_sib)):
         remote(buf.at[z, c], buf.at[z, c], own_sib_out, sib_sem.at[z], tp=sibling).start()
-    begin(*up_args)
 
     @pl.when(home)
     def _():
         for k in range(TOKEN_PARTS):
-            view = pl.ds(k * tok_rows, tok_rows)
-            remote(tok.at[view], other.at[view], tok_out, tok_in.at[k], grp=partner).start()
+            remote(tok.at[token_rows(k)], seen.at[token_rows(k)], tok_out, tok_in.at[k], grp=partner).start()
+
+    begin(*up_args)
+    acc[...] = jnp.zeros_like(acc)
 
     def normalize(k):
+        arrived(seen.at[token_rows(k)], tok_in.at[k])
         step = 32
 
-        def from_rows(src):
-            def body(i, _):
-                view = pl.ds(pl.multiple_of(k * tok_rows + i * step, step), step)
-                values = src[view, :].astype(jnp.float32)
-                mean = jnp.mean(values * values, axis=-1, keepdims=True)
-                scaled = (values * lax.rsqrt(mean + epsilon) * gain[...]).astype(jnp.bfloat16)
-                for q in range(n_quads):
-                    normed[q, view, :] = scaled[:, q * quad : (q + 1) * quad]
-                return 0
-
-            lax.fori_loop(0, tok_rows // step, body, 0)
-
-        @pl.when(home)
-        def _():
-            from_rows(tok)
-
-        @pl.when(jnp.logical_not(home))
-        def _():
-            view = pl.ds(pl.multiple_of(k * tok_rows, tok_rows), tok_rows)
-            arrived(other.at[view], tok_in.at[k])
-            from_rows(other)
+        def body(i, _):
+            view = pl.ds(pl.multiple_of(k * tok_rows + i * step, step), step)
+            values = seen[view, :].astype(jnp.float32)
+            mean = jnp.mean(values * values, axis=-1, keepdims=True)
+            scaled = (values * lax.rsqrt(mean + epsilon) * gain[...]).astype(jnp.bfloat16)
+            for q in range(n_quads):
+                normed[q, view, :] = scaled[:, q * quad : (q + 1) * quad]
+            return 0
+
+        lax.fori_loop(0, tok_rows // step, body, 0)
 
     def lift(m):
         q = lax.rem(z_quad - way * m + n_quads + 8, n_quads)
@@ -153,11 +150,13 @@
             weights = up[pl.ds(4 * q, 4), h].reshape(quad, mine)
             acc[h] += jnp.dot(normed[q], weights, preferred_element_type=jnp.float32)
 
-    norm_at = 8
+    norm_at = 8 + 4 * c
     lift_at = norm_at + TOKEN_PARTS
 
-    def up_pass(s, _):
-        ring_step(s, *up_args)
+    def ring_pass(s, _):
+        @pl.when(s <= last)
+        def _():
+            ring_step(s, *up_args)
 
         @pl.when(s == LAG)
         def _():
@@ -171,13 +170,13 @@
         def _():
             normalize(s - norm_at)
 
-        @pl.when((s == lift_at) | (s == lift_at + 1) | (s == lift_at + 4))
-        def _():
-            lift(jnp.minimum(s - lift_at + 1, 3))
+        @pl.when((s >= lift_at) & (s < lift_at + 2 + c))
+        def _():
+            lift(s - lift_at + 1)
 
         return 0
 
-    lax.fori_loop(1, last + 1, up_pass, 0)
+    lax.fori_loop(1, last + LAG + 1, ring_pass, 0)
 
     def lift_rest(m, _):
         lift(m)
@@ -225,12 +224,12 @@
         view = branch.at[q, own_rows]
         for i in (1, nx - 1):
             remote(view, view, all_out, all_in.at[(nx - 1 - i) * n_quads + j], tp=2 * peer(i) + c).start()
-        remote(view, view, all_sib_out, branch_sib, tp=sibling).start()
+        remote(view, view, all_sib_out, branch_sib.at[j], tp=sibling).start()
 
     def take(i, j):
         view = branch.at[quad_of(j), pl.ds(pl.multiple_of(peer(i) * own, own), own)]
         arrived(view, all_in.at[(i - 1) * n_quads + j])
-        remote(view, view, all_sib_out, branch_sib, tp=sibling).start()
+        remote(view, view, all_sib_out, branch_sib.at[j], tp=sibling).start()
         return view
 
     def hand_on(j):
@@ -240,16 +239,10 @@
 
     def hand_far(j):
         take(2, j)
+        q = quad_of(j)
+        pltpu.make_async_copy(branch.at[q], out.at[q], out_sem.at[j]).start()
 
     def output_pass(i, _):
-        done = last - LAG + PER * i
-
-        def more(s, _):
-            ring_step(s, *down_args)
-            return 0
-
-        lax.fori_loop(jnp.minimum(done, last) + 1, jnp.minimum(done + PER, last) + 1, more, 0)
-
         @pl.when(i < n_quads)
         def _():
             project(i)
@@ -277,7 +270,7 @@
 
     @pl.when(home)
     def _():
-        arrived(tok, tok_out)
+        arrived(seen, tok_out)
         most = part.at[pl.ds(0, n_quads * (nx - 1) // nx)]
         arrived(most, x_out)
         arrived(most, all_out)
@@ -286,25 +279,24 @@
     @pl.when(jnp.logical_not(home))
     def _():
         arrived(part, y_out)
-        arrived(branch, branch_sib)
-
-    step = 32
-
-    def finish(i, _):
-        view = pl.ds(pl.multiple_of(i * step, step), step)
-        squares = jnp.zeros((step, 1), jnp.float32)
-        for q in range(n_quads):
-            values = branch[q, view, :].astype(jnp.float32)
-            squares += jnp.sum(values * values, axis=-1, keepdims=True)
-        scale = lax.rsqrt(squares / width + epsilon)
-        for q in range(n_quads):
-            cols = slice(q * quad, (q + 1) * quad)
-            values = branch[q, view, :].astype(jnp.float32)
-            result = tok[view, cols].astype(jnp.float32) + values * scale * post[:, cols]
-            out[view, cols] = result.astype(jnp.bfloat16)
-        return 0
-
-    lax.fori_loop(0, rows // step, finish, 0)
+        for j in range(n_quads):
+            q = quad_of(j)
+            arrived(branch.at[q], branch_sib.at[j])
+            pltpu.make_async_copy(branch.at[q], out.at[q], out_sem.at[j]).start()
+
+    for j in range(n_quads):
+        arrived(part.at[j], out_sem.at[j])
+
+
+def finish(branch, tok, post, out):
+    n_quads, _, quad = branch.shape
+    values = branch[...].astype(jnp.float32)
+    squares = jnp.sum(jnp.sum(values * values, axis=0), axis=-1, keepdims=True)
+    scale = lax.rsqrt(squares / (n_quads * quad) + epsilon)
+    for q in range(n_quads):
+        cols = slice(q * quad, (q + 1) * quad)
+        result = tok[:, cols].astype(jnp.float32) + values[q] * scale * post[:, cols]
+        out[:, cols] = result.astype(jnp.bfloat16)
 
 
 def solution(mesh):
@@ -320,11 +312,12 @@
         vmem = pl.BlockSpec(memory_space=pltpu.VMEM)
         bf16, f32 = jnp.bfloat16, jnp.float32
         dma = pltpu.SemaphoreType.DMA
-        return pl.pallas_call(
+        anywhere = pl.BlockSpec(memory_space=pl.ANY)
+        branch = pl.pallas_call(
             functools.partial(kernel, nz, nx),
-            out_shape=jax.ShapeDtypeStruct((rows, width), bf16),
-            in_specs=[vmem] * 7,
-            out_specs=vmem,
+            out_shape=jax.ShapeDtypeStruct((n_quads, rows, quad), bf16),
+            in_specs=[anywhere] + [vmem] * 5,
+            out_specs=anywhere,
             scratch_shapes=[
                 pltpu.VMEM((nz, 2, block, mine), bf16),
                 pltpu.VMEM((nz, 2, block, mine), bf16),
@@ -344,17 +337,18 @@
                 dma((n_quads,)),
                 dma(((nx - 1) * n_quads,)),
                 dma(((nx - 1) * n_quads,)),
-                dma,
-                dma,
-                dma,
-                dma,
-                dma,
-                dma,
-                dma,
-                dma,
-                dma,
-                dma,
-                dma,
+                dma((n_quads,)),
+                dma,
+                dma,
+                dma,
+                dma,
+                dma,
+                dma,
+                dma,
+                dma,
+                dma,
+                dma,
+                dma((n_quads,)),
             ],
             compiler_params=pltpu.CompilerParams(
                 collective_id=0, has_side_effects=True, vmem_limit_bytes=60 * 1024 * 1024
@@ -366,8 +360,19 @@
             up_scale.reshape(1, units),
             down_weight.T,
             down_scale.reshape(1, block),
-            post_gain.reshape(1, width),
         )
+        step = rows // 4
+        return pl.pallas_call(
+            finish,
+            grid=(rows // step,),
+            out_shape=jax.ShapeDtypeStruct((rows, width), bf16),
+            in_specs=[
+                pl.BlockSpec((n_quads, step, quad), lambda i: (0, i, 0)),
+                pl.BlockSpec((step, width), lambda i: (i, 0)),
+                pl.BlockSpec((1, width), lambda i: (0, 0)),
+            ],
+            out_specs=pl.BlockSpec((step, width), lambda i: (i, 0)),
+        )(branch, tokens, post_gain.reshape(1, width))
 
     placed = (P(("grp", "fs"), None), P(), P("fs", "tp"), P("tp"), P("tp", "fs"), P("fs"), P())
     return jax.shard_map(

time: 161 us -> 145 us (0.901)
  Pallas kernels: 158 us -> 145 us
  local copies, waits for them, and re-layouts: 3.16 us -> 0 us
    pallas_call x1, Pallas kernels: 158 us -> 140 us  [on_device(): pl.pallas_call(functools.partial(kernel, nz, nx), out_shape=jax.ShapeDtyp...]
    pallas_call x0 -> x1, Pallas kernels: none -> 4.68 us  [on_device(): pl.pallas_call(finish, grid=(rows // step,), out_shape=jax.ShapeDtypeStru...]
    unnamed x1 -> x0, local copies, waits for them, and re-layouts: 3.16 us -> none
where the time goes in v3:
time: 145 us
  Pallas kernels  145 us (100%)
    pallas_call x1, Pallas kernels, on_device(): pl.pallas_call(functools.partial(kernel, nz, nx), out_shape=jax.ShapeDtyp...  140 us
    pallas_call x1, Pallas kernels, on_device(): pl.pallas_call(finish, grid=(rows // step,), out_shape=jax.ShapeDtypeStru...  4.68 us

profile of v3, /device:TPU:33, one launch (start us, length us, event | category | flops | bytes accessed | tf_op | source)
XLA Modules:
  0.0 145.0 jit_solution(3628378962921688259)
XLA Ops:
  0.0 140.3 %shard_map.73.branch = bf16[8,512,256]{2,1,0:T(8,128)(2,1)} custom-call(bf16[512,2048]{1,0:T(8,128)(2,1)} %tok.3, f32[1,2048]{1,0:T(1,128)} %bitcast.6, f32[64,1024]{1,0:T(8,128)} %up_w.1, f32[1,1024]{1,0:T(1,128)} %bitcast.8, f32[64,1024]{1,0:T(8,128)} %bitcast.5, f32[1,64]{1,0:T(1,128)} %bitcast.9), custom_call_target="tpu_custom_call" | custom-call | tf_op jit(solution)/shard_map/pallas_call | solution.py:316
  140.3 4.7 %shard_map.74 = bf16[512,2048]{1,0:T(8,128)(2,1)} custom-call(bf16[8,512,256]{2,1,0:T(8,128)(2,1)} %shard_map.73.branch, bf16[512,2048]{1,0:T(8,128)(2,1)} %tok.3, f32[1,2048]{1,0:T(1,128)} %bitcast.7), custom_call_target="tpu_custom_call" | custom-call | tf_op jit(solution)/shard_map/pallas_call | solution.py:365

commit v4 on v3

--- a/solution.py
+++ b/solution.py
@@ -10,9 +10,10 @@
 epsilon = 1e-06
 MESH = pl.DeviceIdType.MESH
 
-LAG = 2
-PARTS = 2
+LAG = (8, 4)
+PARTS = 4
 TOKEN_PARTS = 4
+LIFTS = ((1, 8, 2, 7, 6, 5, 3, 4), (1, 8, 2, 7, 3, 6, 5, 4))
 ORDER = (1, 2, 0, 3, 7, 4, 6, 5)
 
 
@@ -37,10 +38,12 @@
     mine = units // 2
     quad = 4 * block
     n_quads = width // quad
-    own = rows // nx
+    n_chunks = 2 * n_quads
+    tall = rows // 2
+    own = tall // nx
     tok_rows = rows // TOKEN_PARTS
     piece = block // PARTS
-    reach = (nz * 13 // 32, nz - 1 - nz * 13 // 32)
+    reach = (nz * 12 // 32, nz - 1 - nz * 12 // 32)
 
     g = lax.axis_index("grp")
     z = lax.axis_index("fs")
@@ -56,6 +59,8 @@
     home = c == y
     z_quad = z // 4
     last = jnp.where(c == 0, reach[0], reach[1])
+    lag = jnp.where(c == 0, LAG[0], LAG[1])
+    near = z < nz // 4
 
     def peer(i):
         return lax.rem(x + i, nx)
@@ -81,8 +86,17 @@
     down[z, c] = (down_w[:, half] * column).astype(jnp.bfloat16)
     pl.semaphore_wait(barrier, len(neighbours))
 
+    def pick(values, i):
+        return sum(jnp.where(i == k, v, 0) for k, v in enumerate(values))
+
     def quad_of(j):
-        return lax.rem(z_quad + sum(jnp.where(j == k, ORDER[k], 0) for k in range(n_quads)), n_quads)
+        return lax.rem(z_quad + pick(ORDER, j // 2), n_quads)
+
+    def chunk_rows(j, of=None):
+        first = lax.rem(j, 2) * tall
+        if of is None:
+            return pl.ds(pl.multiple_of(first, tall), tall)
+        return pl.ds(pl.multiple_of(first + of * own, own), own)
 
     def send_half(b, h, buf, in_sem, out_sem, wait):
         for k in range(PARTS):
@@ -143,59 +157,31 @@
 
         lax.fori_loop(0, tok_rows // step, body, 0)
 
-    def lift(m):
+    def lift(i, _):
+        m = jnp.where(c == 0, pick(LIFTS[0], i), pick(LIFTS[1], i))
         q = lax.rem(z_quad - way * m + n_quads + 8, n_quads)
         from_sibling(q, up, up_sib)
         for h in range(2):
             weights = up[pl.ds(4 * q, 4), h].reshape(quad, mine)
             acc[h] += jnp.dot(normed[q], weights, preferred_element_type=jnp.float32)
-
-    norm_at = 8 + 4 * c
-    lift_at = norm_at + TOKEN_PARTS
-
-    def ring_pass(s, _):
-        @pl.when(s <= last)
-        def _():
-            ring_step(s, *up_args)
-
-        @pl.when(s == LAG)
-        def _():
-            begin(*down_args)
-
-        @pl.when(s > LAG)
-        def _():
-            ring_step(s - LAG, *down_args)
-
-        @pl.when((s >= norm_at) & (s < lift_at))
-        def _():
-            normalize(s - norm_at)
-
-        @pl.when((s >= lift_at) & (s < lift_at + 2 + c))
-        def _():
-            lift(s - lift_at + 1)
-
         return 0
 
-    lax.fori_loop(1, last + LAG + 1, ring_pass, 0)
-
-    def lift_rest(m, _):
-        lift(m)
-        return 0
-
-    lax.fori_loop(jnp.where(c == 0, 3, 4), n_quads + 1, lift_rest, 0)
-    for h in range(2):
-        hidden[h] = jnp.square(jnp.maximum(acc[h], 0.0)).astype(jnp.bfloat16)
-
-    own_rows = pl.ds(pl.multiple_of(x * own, own), own)
-
-    def project(j):
+    def activate():
+        for h in range(2):
+            hidden[h] = jnp.square(jnp.maximum(acc[h], 0.0)).astype(jnp.bfloat16)
+
+    def project(j, _):
         q = quad_of(j)
-        from_sibling(q, down, down_sib)
+
+        @pl.when(lax.rem(j, 2) == 0)
+        def _():
+            from_sibling(q, down, down_sib)
+
         total = None
         for h in range(2):
             weights = down[pl.ds(4 * q, 4), h].reshape(quad, mine)
             term = lax.dot_general(
-                hidden[h], weights, (((1,), (1,)), ((), ())), preferred_element_type=jnp.float32
+                hidden[h, chunk_rows(j), :], weights, (((1,), (1,)), ((), ())), preferred_element_type=jnp.float32
             )
             total = term if total is None else total + term
         part[j] = total.astype(jnp.bfloat16)
@@ -203,6 +189,52 @@
         @pl.when(jnp.logical_not(home))
         def _():
             remote(part.at[j], ypart.at[j], y_out, y_in.at[j], grp=partner).start()
+
+        return 0
+
+    norm_at = 7 + 5 * c
+
+    def ring_pass(s, _):
+        @pl.when(s <= last)
+        def _():
+            ring_step(s, *up_args)
+
+        @pl.when(s == lag)
+        def _():
+            begin(*down_args)
+
+        @pl.when(s > lag)
+        def _():
+            ring_step(s - lag, *down_args)
+
+        @pl.when((s >= norm_at) & (s < norm_at + TOKEN_PARTS))
+        def _():
+            normalize(s - norm_at)
+
+        over = s - last
+
+        @pl.when(near & (over >= -1) & (over < 3))
+        def _():
+            lax.fori_loop(2 * over + 2, 2 * over + 4, lift, 0)
+
+        @pl.when(near & (over == 2))
+        def _():
+            activate()
+
+        @pl.when(near & (over >= 3))
+        def _():
+            lax.fori_loop(2 * over - 6, 2 * over - 4, project, 0)
+
+        return 0
+
+    lax.fori_loop(1, last + lag + 1, ring_pass, 0)
+
+    @pl.when(jnp.logical_not(near))
+    def _():
+        lax.fori_loop(0, n_quads, lift, 0)
+        activate()
+
+    made = jnp.where(near, 2 * (lag - 2), 0)
 
     def pair_sum(j):
         arrived(ypart.at[j], y_in.at[j])
@@ -211,53 +243,58 @@
             view = pl.ds(pl.multiple_of(peer(i) * own, own), own)
             slot = nx - 1 - i
             remote(
-                part.at[j, view], xpart.at[slot, j], x_out, x_in.at[slot * n_quads + j], tp=2 * peer(i) + c
+                part.at[j, view], xpart.at[slot, j], x_out, x_in.at[slot * n_chunks + j], tp=2 * peer(i) + c
             ).start()
 
     def row_sum(j):
         q = quad_of(j)
-        total = part[j, own_rows, :].astype(jnp.float32)
+        total = part[j, pl.ds(pl.multiple_of(x * own, own), own), :].astype(jnp.float32)
         for i in range(nx - 1):
-            arrived(xpart.at[i, j], x_in.at[i * n_quads + j])
+            arrived(xpart.at[i, j], x_in.at[i * n_chunks + j])
             total += xpart[i, j].astype(jnp.float32)
-        branch[q, own_rows, :] = total.astype(jnp.bfloat16)
-        view = branch.at[q, own_rows]
+        branch[q, chunk_rows(j, x), :] = total.astype(jnp.bfloat16)
+        view = branch.at[q, chunk_rows(j, x)]
         for i in (1, nx - 1):
-            remote(view, view, all_out, all_in.at[(nx - 1 - i) * n_quads + j], tp=2 * peer(i) + c).start()
+            remote(view, view, all_out, all_in.at[(nx - 1 - i) * n_chunks + j], tp=2 * peer(i) + c).start()
         remote(view, view, all_sib_out, branch_sib.at[j], tp=sibling).start()
 
     def take(i, j):
-        view = branch.at[quad_of(j), pl.ds(pl.multiple_of(peer(i) * own, own), own)]
-        arrived(view, all_in.at[(i - 1) * n_quads + j])
+        view = branch.at[quad_of(j), chunk_rows(j, peer(i))]
+        arrived(view, all_in.at[(i - 1) * n_chunks + j])
         remote(view, view, all_sib_out, branch_sib.at[j], tp=sibling).start()
         return view
 
     def hand_on(j):
         view = take(1, j)
-        remote(view, view, all_out, all_in.at[n_quads + j], tp=2 * peer(nx - 1) + c).start()
+        remote(view, view, all_out, all_in.at[n_chunks + j], tp=2 * peer(nx - 1) + c).start()
         take(nx - 1, j)
+
+    def write(j):
+        view = (quad_of(j), chunk_rows(j))
+        pltpu.make_async_copy(branch.at[view], out.at[view], out_sem.at[j]).start()
 
     def hand_far(j):
         take(2, j)
-        q = quad_of(j)
-        pltpu.make_async_copy(branch.at[q], out.at[q], out_sem.at[j]).start()
+        write(j)
+
+    stages = ((1, pair_sum), (4, row_sum), (7, hand_on), (10, hand_far))
 
     def output_pass(i, _):
-        @pl.when(i < n_quads)
-        def _():
-            project(i)
+        @pl.when(made + i < n_chunks)
+        def _():
+            project(made + i, 0)
 
         @pl.when(home)
         def _():
-            for behind, stage in ((1, pair_sum), (2, row_sum), (3, hand_on), (4, hand_far)):
-
-                @pl.when((i >= behind) & (i < n_quads + behind))
+            for behind, stage in stages:
+
+                @pl.when((i >= behind) & (i < n_chunks + behind))
                 def _():
                     stage(i - behind)
 
         return 0
 
-    lax.fori_loop(0, n_quads + 4, output_pass, 0)
+    lax.fori_loop(0, n_chunks + stages[-1][0], output_pass, 0)
 
     for side in range(2):
 
@@ -271,7 +308,7 @@
     @pl.when(home)
     def _():
         arrived(seen, tok_out)
-        most = part.at[pl.ds(0, n_quads * (nx - 1) // nx)]
+        most = part.at[pl.ds(0, n_chunks * (nx - 1) // nx)]
         arrived(most, x_out)
         arrived(most, all_out)
         arrived(part, all_sib_out)
@@ -279,13 +316,19 @@
     @pl.when(jnp.logical_not(home))
     def _():
         arrived(part, y_out)
-        for j in range(n_quads):
-            q = quad_of(j)
-            arrived(branch.at[q], branch_sib.at[j])
-            pltpu.make_async_copy(branch.at[q], out.at[q], out_sem.at[j]).start()
-
-    for j in range(n_quads):
+
+        def write_arrived(j, _):
+            arrived(part.at[j], branch_sib.at[j])
+            write(j)
+            return 0
+
+        lax.fori_loop(0, n_chunks, write_arrived, 0)
+
+    def written(j, _):
         arrived(part.at[j], out_sem.at[j])
+        return 0
+
+    lax.fori_loop(0, n_chunks, written, 0)
 
 
 def finish(branch, tok, post, out):
@@ -308,7 +351,9 @@
         mine = units // 2
         quad = 4 * block
         n_quads = width // quad
-        own = rows // nx
+        n_chunks = 2 * n_quads
+        tall = rows // 2
+        own = tall // nx
         vmem = pl.BlockSpec(memory_space=pltpu.VMEM)
         bf16, f32 = jnp.bfloat16, jnp.float32
         dma = pltpu.SemaphoreType.DMA
@@ -325,30 +370,30 @@
                 pltpu.VMEM((n_quads, rows, quad), bf16),
                 pltpu.VMEM((2, rows, mine), f32),
                 pltpu.VMEM((2, rows, mine), bf16),
-                pltpu.VMEM((n_quads, rows, quad), bf16),
-                pltpu.VMEM((n_quads, rows, quad), bf16),
-                pltpu.VMEM((nx - 1, n_quads, own, quad), bf16),
+                pltpu.VMEM((n_chunks, tall, quad), bf16),
+                pltpu.VMEM((n_chunks, tall, quad), bf16),
+                pltpu.VMEM((nx - 1, n_chunks, own, quad), bf16),
                 pltpu.VMEM((n_quads, rows, quad), bf16),
                 dma((nz * 2 * PARTS,)),
                 dma((nz * 2 * PARTS,)),
                 dma((nz,)),
                 dma((nz,)),
                 dma((TOKEN_PARTS,)),
-                dma((n_quads,)),
-                dma(((nx - 1) * n_quads,)),
-                dma(((nx - 1) * n_quads,)),
-                dma((n_quads,)),
-                dma,
-                dma,
-                dma,
-                dma,
-                dma,
-                dma,
-                dma,
-                dma,
-                dma,
-                dma,
-                dma((n_quads,)),
+                dma((n_chunks,)),
+                dma(((nx - 1) * n_chunks,)),
+                dma(((nx - 1) * n_chunks,)),
+                dma((n_chunks,)),
+                dma,
+                dma,
+                dma,
+                dma,
+                dma,
+                dma,
+                dma,
+                dma,
+                dma,
+                dma,
+                dma((n_chunks,)),
             ],
             compiler_params=pltpu.CompilerParams(
                 collective_id=0, has_side_effects=True, vmem_limit_bytes=60 * 1024 * 1024
@@ -361,7 +406,7 @@
             down_weight.T,
             down_scale.reshape(1, block),
         )
-        step = rows // 4
+        step = rows // 8
         return pl.pallas_call(
             finish,
             grid=(rows // step,),

time: 145 us -> 143 us (0.986)
  Pallas kernels: 145 us -> 142 us
    pallas_call x1, Pallas kernels: 140 us -> 135 us  [on_device(): pl.pallas_call(functools.partial(kernel, nz, nx), out_shape=jax.ShapeDtyp...]
    pallas_call x1, Pallas kernels: 4.68 us -> 6.7 us  [on_device(): pl.pallas_call(finish, grid=(rows // step,), out_shape=jax.ShapeDtypeStru...]
where the time goes in v4:
time: 143 us; the launch traced here: 142 us
  Pallas kernels  142 us (99%)
    pallas_call x1, Pallas kernels, on_device(): pl.pallas_call(functools.partial(kernel, nz, nx), out_shape=jax.ShapeDtyp...  135 us
    pallas_call x1, Pallas kernels, on_device(): pl.pallas_call(finish, grid=(rows // step,), out_shape=jax.ShapeDtypeStru...  6.7 us

profile of v4, /device:TPU:33, one launch (start us, length us, event | category | flops | bytes accessed | tf_op | source)
XLA Modules:
  0.0 141.9 jit_solution(14330147094031440977)
XLA Ops:
  0.0 135.2 %shard_map.73.branch = bf16[8,512,256]{2,1,0:T(8,128)(2,1)} custom-call(bf16[512,2048]{1,0:T(8,128)(2,1)} %tok.3, f32[1,2048]{1,0:T(1,128)} %bitcast.6, f32[64,1024]{1,0:T(8,128)} %up_w.1, f32[1,1024]{1,0:T(1,128)} %bitcast.8, f32[64,1024]{1,0:T(8,128)} %bitcast.5, f32[1,64]{1,0:T(1,128)} %bitcast.9), custom_call_target="tpu_custom_call" | custom-call | tf_op jit(solution)/shard_map/pallas_call | solution.py:361
  135.2 6.7 %shard_map.74 = bf16[512,2048]{1,0:T(8,128)(2,1)} custom-call(bf16[8,512,256]{2,1,0:T(8,128)(2,1)} %shard_map.73.branch, bf16[512,2048]{1,0:T(8,128)(2,1)} %tok.3, f32[1,2048]{1,0:T(1,128)} %bitcast.7), custom_call_target="tpu_custom_call" | custom-call | tf_op jit(solution)/shard_map/pallas_call | solution.py:410

commit v5 on v4

--- a/solution.py
+++ b/solution.py
@@ -11,7 +11,8 @@
 MESH = pl.DeviceIdType.MESH
 
 LAG = (8, 4)
-PARTS = 4
+UP_PARTS, DOWN_PARTS = 4, 2
+TICKS = (5, 3)
 TOKEN_PARTS = 4
 LIFTS = ((1, 8, 2, 7, 6, 5, 3, 4), (1, 8, 2, 7, 3, 6, 5, 4))
 ORDER = (1, 2, 0, 3, 7, 4, 6, 5)
@@ -27,10 +28,14 @@
     pltpu.make_async_copy(ref, ref, sem).wait()
 
 
+def reaches(nz):
+    return nz * 12 // 32, nz - 1 - nz * 12 // 32
+
+
 def kernel(
     nz, nx, tok, gain, up_w, up_s, down_w, down_s, out,
     up, down, seen, normed, acc, hidden, part, ypart, xpart, branch,
-    up_in, down_in, up_sib, down_sib, tok_in, y_in, x_in, all_in, branch_sib,
+    up_in, down_in, up_sib, down_sib, own_sib, tok_in, y_in, x_in, all_in, branch_sib,
     up_out, down_out, up_sib_out, down_sib_out, own_sib_out, tok_out, y_out, x_out, all_out, all_sib_out, out_sem,
 ):
     rows, width = tok.shape
@@ -42,8 +47,7 @@
     tall = rows // 2
     own = tall // nx
     tok_rows = rows // TOKEN_PARTS
-    piece = block // PARTS
-    reach = (nz * 12 // 32, nz - 1 - nz * 12 // 32)
+    reach = reaches(nz)
 
     g = lax.axis_index("grp")
     z = lax.axis_index("fs")
@@ -60,7 +64,7 @@
     z_quad = z // 4
     last = jnp.where(c == 0, reach[0], reach[1])
     lag = jnp.where(c == 0, LAG[0], LAG[1])
-    near = z < nz // 4
+    near = z < nz // 2
 
     def peer(i):
         return lax.rem(x + i, nx)
@@ -98,41 +102,50 @@
             return pl.ds(pl.multiple_of(first, tall), tall)
         return pl.ds(pl.multiple_of(first + of * own, own), own)
 
-    def send_half(b, h, buf, in_sem, out_sem, wait):
-        for k in range(PARTS):
+    def send_half(s, b, h, buf, in_sem, out_sem, parts):
+        piece = block // parts
+        for k in range(parts):
             view = buf.at[b, h, pl.ds(k * piece, piece)]
-            sem = in_sem.at[(2 * b + h) * PARTS + k]
-            if wait is not None:
-                arrived(view, sem)
-
-            @pl.when(True if wait is None else wait)
+
+            def slot(step):
+                return in_sem.at[(2 * (step - 1) + h) * parts + k]
+
+            if s is None:
+                remote(view, view, out_sem, slot(1), fs=following).start()
+                continue
+            arrived(view, slot(s))
+
+            @pl.when(s < last)
             def _():
-                remote(view, view, out_sem, sem, fs=following).start()
-
-    def begin(buf, in_sem, sib_sem, out_sem, sib_out):
-        send_half(z, c, buf, in_sem, out_sem, None)
-        arrived(buf.at[z, 1 - c], sib_sem.at[z])
-        send_half(z, 1 - c, buf, in_sem, out_sem, None)
-
-    def ring_step(s, buf, in_sem, sib_sem, out_sem, sib_out):
+                remote(view, view, out_sem, slot(s + 1), fs=following).start()
+
+    def begin(buf, in_sem, sib_sem, out_sem, sib_out, own_sem, parts):
+        send_half(None, z, c, buf, in_sem, out_sem, parts)
+        arrived(buf.at[z, 1 - c], own_sem)
+        send_half(None, z, 1 - c, buf, in_sem, out_sem, parts)
+
+    def ring_step(s, buf, in_sem, sib_sem, out_sem, sib_out, own_sem, parts):
         b = lax.rem(z - way * s + nz, nz)
         for h in (c, 1 - c):
-            send_half(b, h, buf, in_sem, out_sem, s < last)
-        remote(buf.at[b], buf.at[b], sib_out, sib_sem.at[b], tp=sibling).start()
+            send_half(s, b, h, buf, in_sem, out_sem, parts)
+        remote(buf.at[b], buf.at[b], sib_out, sib_sem.at[b // 4], tp=sibling).start()
 
     def from_sibling(q, buf, sib_sem):
+        count = 0
         for i in range(4):
-            b = 4 * q + i
-            ahead = lax.rem(b - z + nz, nz)
-
-            @pl.when((ahead > 0) & jnp.where(c == 0, ahead <= reach[1], ahead > reach[1]))
+            ahead = lax.rem(4 * q + i - z + nz, nz)
+            theirs = (ahead > 0) & jnp.where(c == 0, ahead <= reach[1], ahead > reach[1])
+            count += jnp.where(theirs, 1, 0)
+        for n in range(1, 5):
+
+            @pl.when(count == n)
             def _():
-                arrived(buf.at[b], sib_sem.at[b])
-
-    up_args = (up, up_in, up_sib, up_out, up_sib_out)
-    down_args = (down, down_in, down_sib, down_out, down_sib_out)
-    for buf, sib_sem in ((up, up_sib), (down, down_sib)):
-        remote(buf.at[z, c], buf.at[z, c], own_sib_out, sib_sem.at[z], tp=sibling).start()
+                arrived(buf.at[pl.ds(0, n)], sib_sem.at[q])
+
+    up_args = (up, up_in, up_sib, up_out, up_sib_out, own_sib.at[0], UP_PARTS)
+    down_args = (down, down_in, down_sib, down_out, down_sib_out, own_sib.at[1], DOWN_PARTS)
+    for k, buf in enumerate((up, down)):
+        remote(buf.at[z, c], buf.at[z, c], own_sib_out, own_sib.at[k], tp=sibling).start()
 
     @pl.when(home)
     def _():
@@ -192,50 +205,6 @@
 
         return 0
 
-    norm_at = 7 + 5 * c
-
-    def ring_pass(s, _):
-        @pl.when(s <= last)
-        def _():
-            ring_step(s, *up_args)
-
-        @pl.when(s == lag)
-        def _():
-            begin(*down_args)
-
-        @pl.when(s > lag)
-        def _():
-            ring_step(s - lag, *down_args)
-
-        @pl.when((s >= norm_at) & (s < norm_at + TOKEN_PARTS))
-        def _():
-            normalize(s - norm_at)
-
-        over = s - last
-
-        @pl.when(near & (over >= -1) & (over < 3))
-        def _():
-            lax.fori_loop(2 * over + 2, 2 * over + 4, lift, 0)
-
-        @pl.when(near & (over == 2))
-        def _():
-            activate()
-
-        @pl.when(near & (over >= 3))
-        def _():
-            lax.fori_loop(2 * over - 6, 2 * over - 4, project, 0)
-
-        return 0
-
-    lax.fori_loop(1, last + lag + 1, ring_pass, 0)
-
-    @pl.when(jnp.logical_not(near))
-    def _():
-        lax.fori_loop(0, n_quads, lift, 0)
-        activate()
-
-    made = jnp.where(near, 2 * (lag - 2), 0)
-
     def pair_sum(j):
         arrived(ypart.at[j], y_in.at[j])
         part[j] = (part[j].astype(jnp.float32) + ypart[j].astype(jnp.float32)).astype(jnp.bfloat16)
@@ -243,41 +212,110 @@
             view = pl.ds(pl.multiple_of(peer(i) * own, own), own)
             slot = nx - 1 - i
             remote(
-                part.at[j, view], xpart.at[slot, j], x_out, x_in.at[slot * n_chunks + j], tp=2 * peer(i) + c
+                part.at[j, view], xpart.at[j, slot], x_out, x_in.at[j], tp=2 * peer(i) + c
             ).start()
 
     def row_sum(j):
         q = quad_of(j)
         total = part[j, pl.ds(pl.multiple_of(x * own, own), own), :].astype(jnp.float32)
+        arrived(xpart.at[j], x_in.at[j])
         for i in range(nx - 1):
-            arrived(xpart.at[i, j], x_in.at[i * n_chunks + j])
-            total += xpart[i, j].astype(jnp.float32)
+            total += xpart[j, i].astype(jnp.float32)
         branch[q, chunk_rows(j, x), :] = total.astype(jnp.bfloat16)
         view = branch.at[q, chunk_rows(j, x)]
         for i in (1, nx - 1):
-            remote(view, view, all_out, all_in.at[(nx - 1 - i) * n_chunks + j], tp=2 * peer(i) + c).start()
+            remote(view, view, all_out, all_in.at[j], tp=2 * peer(i) + c).start()
         remote(view, view, all_sib_out, branch_sib.at[j], tp=sibling).start()
 
-    def take(i, j):
+    def pass_on(i, j):
         view = branch.at[quad_of(j), chunk_rows(j, peer(i))]
-        arrived(view, all_in.at[(i - 1) * n_chunks + j])
         remote(view, view, all_sib_out, branch_sib.at[j], tp=sibling).start()
         return view
 
     def hand_on(j):
-        view = take(1, j)
+        arrived(part.at[j, pl.ds(0, 2 * own)], all_in.at[j])
+        view = pass_on(1, j)
         remote(view, view, all_out, all_in.at[n_chunks + j], tp=2 * peer(nx - 1) + c).start()
-        take(nx - 1, j)
+        pass_on(nx - 1, j)
 
     def write(j):
         view = (quad_of(j), chunk_rows(j))
-        pltpu.make_async_copy(branch.at[view], out.at[view], out_sem.at[j]).start()
+        pltpu.make_async_copy(branch.at[view], out.at[view], out_sem).start()
 
     def hand_far(j):
-        take(2, j)
+        arrived(part.at[j, pl.ds(0, own)], all_in.at[n_chunks + j])
+        pass_on(2, j)
         write(j)
 
     stages = ((1, pair_sum), (4, row_sum), (7, hand_on), (10, hand_far))
+
+    def tick(i, _):
+        for behind, stage in stages:
+
+            @pl.when((i >= behind) & (i < n_chunks + behind))
+            def _():
+                stage(i - behind)
+
+        return 0
+
+    ready = jnp.where(c == 0, 2, 0)
+    ticks_at = jnp.where(c == 0, TICKS[0], TICKS[1])
+
+    def lifts_at(over):
+        return jnp.clip(2 * over + 2, 0, n_quads) * (1 - c) + jnp.where(
+            over > 0, n_quads, jnp.clip(2 * over + 4, 0, n_quads)
+        ) * c
+
+    norm_at = 7 + 5 * c
+
+    def ring_pass(s, _):
+        @pl.when(s <= last)
+        def _():
+            ring_step(s, *up_args)
+
+        @pl.when(s == lag)
+        def _():
+            begin(*down_args)
+
+        @pl.when(s > lag)
+        def _():
+            ring_step(s - lag, *down_args)
+
+        @pl.when((s >= norm_at) & (s < norm_at + TOKEN_PARTS))
+        def _():
+            normalize(s - norm_at)
+
+        over = s - last
+
+        lo, hi = lifts_at(over), lifts_at(over + 1)
+
+        @pl.when(near & (hi > lo))
+        def _():
+            lax.fori_loop(lo, hi, lift, 0)
+
+        @pl.when(near & (over == ready))
+        def _():
+            activate()
+
+        @pl.when(near & (over > ready))
+        def _():
+            lax.fori_loop(2 * (over - ready) - 2, 2 * (over - ready), project, 0)
+
+        @pl.when(near & home & (over >= ticks_at))
+        def _():
+            lax.fori_loop(2 * (over - ticks_at) + 1, 2 * (over - ticks_at) + 3, tick, 0)
+
+        return 0
+
+    lax.fori_loop(1, last + lag + 1, ring_pass, 0)
+
+    @pl.when(jnp.logical_not(near))
+    def _():
+        lax.fori_loop(0, n_quads, lift, 0)
+        activate()
+
+    made = jnp.where(near, 2 * (lag - ready), 0)
+    ticked = jnp.where(near, 2 * (lag - ticks_at + 1) + 1, 0)
 
     def output_pass(i, _):
         @pl.when(made + i < n_chunks)
@@ -286,11 +324,7 @@
 
         @pl.when(home)
         def _():
-            for behind, stage in stages:
-
-                @pl.when((i >= behind) & (i < n_chunks + behind))
-                def _():
-                    stage(i - behind)
+            tick(ticked + i, 0)
 
         return 0
 
@@ -324,11 +358,7 @@
 
         lax.fori_loop(0, n_chunks, write_arrived, 0)
 
-    def written(j, _):
-        arrived(part.at[j], out_sem.at[j])
-        return 0
-
-    lax.fori_loop(0, n_chunks, written, 0)
+    arrived(part, out_sem)
 
 
 def finish(branch, tok, post, out):
@@ -354,6 +384,7 @@
         n_chunks = 2 * n_quads
         tall = rows // 2
         own = tall // nx
+        longest = max(reaches(nz))
         vmem = pl.BlockSpec(memory_space=pltpu.VMEM)
         bf16, f32 = jnp.bfloat16, jnp.float32
         dma = pltpu.SemaphoreType.DMA
@@ -372,28 +403,29 @@
                 pltpu.VMEM((2, rows, mine), bf16),
                 pltpu.VMEM((n_chunks, tall, quad), bf16),
                 pltpu.VMEM((n_chunks, tall, quad), bf16),
-                pltpu.VMEM((nx - 1, n_chunks, own, quad), bf16),
+                pltpu.VMEM((n_chunks, nx - 1, own, quad), bf16),
                 pltpu.VMEM((n_quads, rows, quad), bf16),
-                dma((nz * 2 * PARTS,)),
-                dma((nz * 2 * PARTS,)),
-                dma((nz,)),
-                dma((nz,)),
+                dma((longest * 2 * UP_PARTS,)),
+                dma((longest * 2 * DOWN_PARTS,)),
+                dma((n_quads,)),
+                dma((n_quads,)),
+                dma((2,)),
                 dma((TOKEN_PARTS,)),
                 dma((n_chunks,)),
-                dma(((nx - 1) * n_chunks,)),
-                dma(((nx - 1) * n_chunks,)),
                 dma((n_chunks,)),
-                dma,
-                dma,
-                dma,
-                dma,
-                dma,
-                dma,
-                dma,
-                dma,
-                dma,
-                dma,
+                dma((2 * n_chunks,)),
                 dma((n_chunks,)),
+                dma,
+                dma,
+                dma,
+                dma,
+                dma,
+                dma,
+                dma,
+                dma,
+                dma,
+                dma,
+                dma,
             ],
             compiler_params=pltpu.CompilerParams(
                 collective_id=0, has_side_effects=True, vmem_limit_bytes=60 * 1024 * 1024

time: 143 us -> 135 us (0.944)
  Pallas kernels: 142 us -> 134 us
    pallas_call x1, Pallas kernels: 135 us -> 128 us  [on_device(): pl.pallas_call(functools.partial(kernel, nz, nx), out_shape=jax.ShapeDtyp...]
where the time goes in v5:
time: 135 us; the launch traced here: 134 us
  Pallas kernels  134 us (99%)
    pallas_call x1, Pallas kernels, on_device(): pl.pallas_call(functools.partial(kernel, nz, nx), out_shape=jax.ShapeDtyp...  128 us
    pallas_call x1, Pallas kernels, on_device(): pl.pallas_call(finish, grid=(rows // step,), out_shape=jax.ShapeDtypeStru...  6.7 us

profile of v5, /device:TPU:33, one launch (start us, length us, event | category | flops | bytes accessed | tf_op | source)
XLA Modules:
  0.0 134.4 jit_solution(4371719788744734975)
XLA Ops:
  0.0 127.7 %shard_map.73.branch = bf16[8,512,256]{2,1,0:T(8,128)(2,1)} custom-call(bf16[512,2048]{1,0:T(8,128)(2,1)} %tok.3, f32[1,2048]{1,0:T(1,128)} %bitcast.6, f32[64,1024]{1,0:T(8,128)} %up_w.1, f32[1,1024]{1,0:T(1,128)} %bitcast.8, f32[64,1024]{1,0:T(8,128)} %bitcast.5, f32[1,64]{1,0:T(1,128)} %bitcast.9), custom_call_target="tpu_custom_call" | custom-call | tf_op jit(solution)/shard_map/pallas_call | solution.py:392
  127.7 6.7 %shard_map.74 = bf16[512,2048]{1,0:T(8,128)(2,1)} custom-call(bf16[8,512,256]{2,1,0:T(8,128)(2,1)} %shard_map.73.branch, bf16[512,2048]{1,0:T(8,128)(2,1)} %tok.3, f32[1,2048]{1,0:T(1,128)} %bitcast.7), custom_call_target="tpu_custom_call" | custom-call | tf_op jit(solution)/shard_map/pallas_call | solution.py:442

commit v6 on v5

--- a/solution.py
+++ b/solution.py
@@ -10,12 +10,12 @@
 epsilon = 1e-06
 MESH = pl.DeviceIdType.MESH
 
-LAG = (8, 4)
+LAG = (8, 6)
 UP_PARTS, DOWN_PARTS = 4, 2
 TICKS = (5, 3)
 TOKEN_PARTS = 4
 LIFTS = ((1, 8, 2, 7, 6, 5, 3, 4), (1, 8, 2, 7, 3, 6, 5, 4))
-ORDER = (1, 2, 0, 3, 7, 4, 6, 5)
+ORDER = (1, 2, 0, 3, 7, 6, 4, 5)
 
 
 def remote(src, dst, send_sem, recv_sem, **where):
@@ -29,17 +29,17 @@
 
 
 def reaches(nz):
-    return nz * 12 // 32, nz - 1 - nz * 12 // 32
+    return nz * 13 // 32, nz - 1 - nz * 13 // 32
 
 
 def kernel(
-    nz, nx, tok, gain, up_w, up_s, down_w, down_s, out,
-    up, down, seen, normed, acc, hidden, part, ypart, xpart, branch,
+    nz, nx, tok, gain_in, up_w_in, up_s_in, down_w_in, down_s_in, out, scale_out,
+    gain, up_w, up_s, down_w, down_s, squares, up, down, seen, normed, acc, hidden, part, ypart, xpart, branch,
     up_in, down_in, up_sib, down_sib, own_sib, tok_in, y_in, x_in, all_in, branch_sib,
-    up_out, down_out, up_sib_out, down_sib_out, own_sib_out, tok_out, y_out, x_out, all_out, all_sib_out, out_sem,
+    up_out, down_out, up_sib_out, down_sib_out, own_sib_out, tok_out, y_out, x_out, all_out, all_sib_out, out_sem, fetched, scale_sem,
 ):
     rows, width = tok.shape
-    block, units = up_w.shape
+    block, units = up_w_in.shape
     mine = units // 2
     quad = 4 * block
     n_quads = width // quad
@@ -69,6 +69,14 @@
     def peer(i):
         return lax.rem(x + i, nx)
 
+    fetches = [
+        pltpu.make_async_copy(src, dst, fetched.at[k])
+        for k, (src, dst) in enumerate(
+            ((up_w_in, up_w), (up_s_in, up_s), (down_w_in, down_w), (down_s_in, down_s), (gain_in, gain))
+        )
+    ]
+    for fetch in fetches:
+        fetch.start()
     barrier = pltpu.get_barrier_semaphore()
     neighbours = [{"fs": previous}, {"tp": sibling}, {"grp": partner}]
     neighbours += [{"tp": 2 * peer(i) + c} for i in range(1, nx)]
@@ -83,6 +91,8 @@
         for k in range(TOKEN_PARTS):
             pltpu.make_async_copy(tok.at[token_rows(k)], seen.at[token_rows(k)], tok_in.at[k]).start()
 
+    for fetch in fetches:
+        fetch.wait()
     half = pl.ds(pl.multiple_of(y * mine, mine), mine)
     up[z, c] = (up_w[:, half] * up_s[:, half]).astype(jnp.bfloat16)
     line = lax.broadcasted_iota(jnp.int32, (block, block), 0) == lax.broadcasted_iota(jnp.int32, (block, block), 1)
@@ -154,6 +164,7 @@
 
     begin(*up_args)
     acc[...] = jnp.zeros_like(acc)
+    squares[...] = jnp.zeros_like(squares)
 
     def normalize(k):
         arrived(seen.at[token_rows(k)], tok_in.at[k])
@@ -241,6 +252,10 @@
     def write(j):
         view = (quad_of(j), chunk_rows(j))
         pltpu.make_async_copy(branch.at[view], out.at[view], out_sem).start()
+        values = branch[view[0], view[1], :].astype(jnp.float32)
+        values *= values
+        lanes = squares.shape[1]
+        squares[view[1], :] += sum(values[:, k : k + lanes] for k in range(0, quad, lanes))
 
     def hand_far(j):
         arrived(part.at[j, pl.ds(0, own)], all_in.at[n_chunks + j])
@@ -266,7 +281,7 @@
             over > 0, n_quads, jnp.clip(2 * over + 4, 0, n_quads)
         ) * c
 
-    norm_at = 7 + 5 * c
+    norm_at = 8 + 3 * c
 
     def ring_pass(s, _):
         @pl.when(s <= last)
@@ -358,18 +373,22 @@
 
         lax.fori_loop(0, n_chunks, write_arrived, 0)
 
+    total = jnp.sum(squares[...], axis=-1, keepdims=True)
+    squares[...] = jnp.broadcast_to(lax.rsqrt(total / width + epsilon), squares.shape)
+    written = pltpu.make_async_copy(squares, scale_out, scale_sem)
+    written.start()
     arrived(part, out_sem)
-
-
-def finish(branch, tok, post, out):
+    written.wait()
+
+
+def finish(branch, scale, tok, post, out):
     n_quads, _, quad = branch.shape
-    values = branch[...].astype(jnp.float32)
-    squares = jnp.sum(jnp.sum(values * values, axis=0), axis=-1, keepdims=True)
-    scale = lax.rsqrt(squares / (n_quads * quad) + epsilon)
+    lanes = scale.shape[1]
     for q in range(n_quads):
-        cols = slice(q * quad, (q + 1) * quad)
-        result = tok[:, cols].astype(jnp.float32) + values[q] * scale * post[:, cols]
-        out[:, cols] = result.astype(jnp.bfloat16)
+        for k in range(0, quad, lanes):
+            cols = slice(q * quad + k, q * quad + k + lanes)
+            values = branch[q, :, k : k + lanes].astype(jnp.float32) * scale[...] * post[:, cols]
+            out[:, cols] = (tok[:, cols].astype(jnp.float32) + values).astype(jnp.bfloat16)
 
 
 def solution(mesh):
@@ -385,16 +404,24 @@
         tall = rows // 2
         own = tall // nx
         longest = max(reaches(nz))
-        vmem = pl.BlockSpec(memory_space=pltpu.VMEM)
         bf16, f32 = jnp.bfloat16, jnp.float32
         dma = pltpu.SemaphoreType.DMA
         anywhere = pl.BlockSpec(memory_space=pl.ANY)
-        branch = pl.pallas_call(
+        branch, scale = pl.pallas_call(
             functools.partial(kernel, nz, nx),
-            out_shape=jax.ShapeDtypeStruct((n_quads, rows, quad), bf16),
-            in_specs=[anywhere] + [vmem] * 5,
-            out_specs=anywhere,
+            out_shape=(
+                jax.ShapeDtypeStruct((n_quads, rows, quad), bf16),
+                jax.ShapeDtypeStruct((rows, 128), f32),
+            ),
+            in_specs=[anywhere] * 6,
+            out_specs=(anywhere, anywhere),
             scratch_shapes=[
+                pltpu.VMEM((1, width), f32),
+                pltpu.VMEM((block, units), f32),
+                pltpu.VMEM((1, units), f32),
+                pltpu.VMEM((block, units), f32),
+                pltpu.VMEM((1, block), f32),
+                pltpu.VMEM((rows, 128), f32),
                 pltpu.VMEM((nz, 2, block, mine), bf16),
                 pltpu.VMEM((nz, 2, block, mine), bf16),
                 pltpu.VMEM((rows, width), bf16),
@@ -426,6 +453,8 @@
                 dma,
                 dma,
                 dma,
+                dma((5,)),
+                dma,
             ],
             compiler_params=pltpu.CompilerParams(
                 collective_id=0, has_side_effects=True, vmem_limit_bytes=60 * 1024 * 1024
@@ -445,11 +474,12 @@
             out_shape=jax.ShapeDtypeStruct((rows, width), bf16),
             in_specs=[
                 pl.BlockSpec((n_quads, step, quad), lambda i: (0, i, 0)),
+                pl.BlockSpec((step, 128), lambda i: (i, 0)),
                 pl.BlockSpec((step, width), lambda i: (i, 0)),
                 pl.BlockSpec((1, width), lambda i: (0, 0)),
             ],
             out_specs=pl.BlockSpec((step, width), lambda i: (i, 0)),
-        )(branch, tokens, post_gain.reshape(1, width))
+        )(branch, scale, tokens, post_gain.reshape(1, width))
 
     placed = (P(("grp", "fs"), None), P(), P("fs", "tp"), P("tp"), P("tp", "fs"), P("fs"), P())
     return jax.shard_map(

time: 135 us -> 136 us (level)
  Pallas kernels: 134 us -> 136 us
    pallas_call x1, Pallas kernels: 128 us -> 130 us  [on_device(): pl.pallas_call(functools.partial(kernel, nz, nx), out_shape=(jax.ShapeDty...]
where the time goes in v6:
time: 136 us
  Pallas kernels  136 us (100%)
    pallas_call x1, Pallas kernels, on_device(): pl.pallas_call(functools.partial(kernel, nz, nx), out_shape=(jax.ShapeDty...  130 us
    pallas_call x1, Pallas kernels, on_device(): pl.pallas_call(finish, grid=(rows // step,), out_shape=jax.ShapeDtypeStru...  6.45 us

profile of v6, /device:TPU:33, one launch (start us, length us, event | category | flops | bytes accessed | tf_op | source)
XLA Modules:
  0.0 136.2 jit_solution(10860024006996984413)
XLA Ops:
  0.0 129.7 %shard_map.73 = (bf16[8,512,256]{2,1,0:T(8,128)(2,1)}, f32[512,128]{1,0:T(8,128)}) custom-call(bf16[512,2048]{1,0:T(8,128)(2,1)} %tok.3, f32[1,2048]{1,0:T(1,128)} %bitcast.6, f32[64,1024]{1,0:T(8,128)} %up_w_in.1, f32[1,1024]{1,0:T(1,128)} %bitcast.8, f32[64,1024]{1,0:T(8,128)} %bitcast.5, f32[1,64]{1,0:T(1,128)} %bitcast.9), custom_call_target="tpu_custom_call" | custom-call | tf_op jit(solution)/shard_map/pallas_call | solution.py:410
  129.7 6.5 %shard_map.74 = bf16[512,2048]{1,0:T(8,128)(2,1)} custom-call(bf16[8,512,256]{2,1,0:T(8,128)(2,1)} %get-tuple-element.7.branch, f32[512,128]{1,0:T(8,128)} %get-tuple-element.8.scale, bf16[512,2048]{1,0:T(8,128)(2,1)} %tok.3, f32[1,2048]{1,0:T(1,128)} %bitcast.7), custom_call_target="tpu_custom_call" | custom-call | tf_op jit(solution)/shard_map/pallas_call | solution.py:471

commit v7 on v6

--- a/solution.py
+++ b/solution.py
@@ -12,8 +12,9 @@
 
 LAG = (8, 6)
 UP_PARTS, DOWN_PARTS = 4, 2
-TICKS = (5, 3)
+TICKS = (4, 2)
 TOKEN_PARTS = 4
+FINISH_PARTS = 4
 LIFTS = ((1, 8, 2, 7, 6, 5, 3, 4), (1, 8, 2, 7, 3, 6, 5, 4))
 ORDER = (1, 2, 0, 3, 7, 6, 4, 5)
 
@@ -64,7 +65,7 @@
     z_quad = z // 4
     last = jnp.where(c == 0, reach[0], reach[1])
     lag = jnp.where(c == 0, LAG[0], LAG[1])
-    near = z < nz // 2
+    near = (z < nz // 2) | (c == 1)
 
     def peer(i):
         return lax.rem(x + i, nx)
@@ -273,13 +274,11 @@
 
         return 0
 
-    ready = jnp.where(c == 0, 2, 0)
+    ready = jnp.where(c == 0, 1, 0)
     ticks_at = jnp.where(c == 0, TICKS[0], TICKS[1])
 
     def lifts_at(over):
-        return jnp.clip(2 * over + 2, 0, n_quads) * (1 - c) + jnp.where(
-            over > 0, n_quads, jnp.clip(2 * over + 4, 0, n_quads)
-        ) * c
+        return jnp.where((c == 1) & (over > 0), n_quads, jnp.clip(2 * over + 4, 0, n_quads))
 
     norm_at = 8 + 3 * c
 
@@ -381,14 +380,36 @@
     written.wait()
 
 
-def finish(branch, scale, tok, post, out):
-    n_quads, _, quad = branch.shape
+def finish(branch, scale, tok, post, out, branch_v, scale_v, tok_v, out_v, came, left):
+    n_quads, rows, quad = branch.shape
     lanes = scale.shape[1]
-    for q in range(n_quads):
-        for k in range(0, quad, lanes):
-            cols = slice(q * quad + k, q * quad + k + lanes)
-            values = branch[q, :, k : k + lanes].astype(jnp.float32) * scale[...] * post[:, cols]
-            out[:, cols] = (tok[:, cols].astype(jnp.float32) + values).astype(jnp.bfloat16)
+    tall = rows // FINISH_PARTS
+
+    def reads(k):
+        view = pl.ds(k * tall, tall)
+        return [
+            pltpu.make_async_copy(branch.at[:, view], branch_v.at[:, view], came.at[3 * k]),
+            pltpu.make_async_copy(scale.at[view], scale_v.at[view], came.at[3 * k + 1]),
+            pltpu.make_async_copy(tok.at[view], tok_v.at[view], came.at[3 * k + 2]),
+        ]
+
+    for k in range(FINISH_PARTS):
+        for copy in reads(k):
+            copy.start()
+    writes = []
+    for k in range(FINISH_PARTS):
+        view = slice(k * tall, (k + 1) * tall)
+        for copy in reads(k):
+            copy.wait()
+        for q in range(n_quads):
+            for i in range(0, quad, lanes):
+                cols = slice(q * quad + i, q * quad + i + lanes)
+                values = branch_v[q, view, i : i + lanes].astype(jnp.float32) * scale_v[view, :] * post[:, cols]
+                out_v[view, cols] = (tok_v[view, cols].astype(jnp.float32) + values).astype(jnp.bfloat16)
+        writes.append(pltpu.make_async_copy(out_v.at[view], out.at[view], left.at[k]))
+        writes[-1].start()
+    for copy in writes:
+        copy.wait()
 
 
 def solution(mesh):
@@ -467,18 +488,20 @@
             down_weight.T,
             down_scale.reshape(1, block),
         )
-        step = rows // 8
         return pl.pallas_call(
             finish,
-            grid=(rows // step,),
             out_shape=jax.ShapeDtypeStruct((rows, width), bf16),
-            in_specs=[
-                pl.BlockSpec((n_quads, step, quad), lambda i: (0, i, 0)),
-                pl.BlockSpec((step, 128), lambda i: (i, 0)),
-                pl.BlockSpec((step, width), lambda i: (i, 0)),
-                pl.BlockSpec((1, width), lambda i: (0, 0)),
+            in_specs=[anywhere] * 3 + [pl.BlockSpec(memory_space=pltpu.VMEM)],
+            out_specs=anywhere,
+            scratch_shapes=[
+                pltpu.VMEM((n_quads, rows, quad), bf16),
+                pltpu.VMEM((rows, 128), f32),
+                pltpu.VMEM((rows, width), bf16),
+                pltpu.VMEM((rows, width), bf16),
+                dma((3 * FINISH_PARTS,)),
+                dma((FINISH_PARTS,)),
             ],
-            out_specs=pl.BlockSpec((step, width), lambda i: (i, 0)),
+            compiler_params=pltpu.CompilerParams(vmem_limit_bytes=60 * 1024 * 1024),
         )(branch, scale, tokens, post_gain.reshape(1, width))
 
     placed = (P(("grp", "fs"), None), P(), P("fs", "tp"), P("tp"), P("tp", "fs"), P("fs"), P())

time: 136 us -> 131 us (0.963)
  Pallas kernels: 136 us -> 131 us
    pallas_call x1, Pallas kernels: 130 us -> 127 us  [on_device(): pl.pallas_call(functools.partial(kernel, nz, nx), out_shape=(jax.ShapeDty...]
    pallas_call x1, Pallas kernels: 6.45 us -> 4.06 us  [on_device(): pl.pallas_call(finish, out_shape=jax.ShapeDtypeStruct((rows, width), bf16...]
where the time goes in v7:
time: 131 us
  Pallas kernels  131 us (100%)
    pallas_call x1, Pallas kernels, on_device(): pl.pallas_call(functools.partial(kernel, nz, nx), out_shape=(jax.ShapeDty...  127 us
    pallas_call x1, Pallas kernels, on_device(): pl.pallas_call(finish, out_shape=jax.ShapeDtypeStruct((rows, width), bf16...  4.06 us

profile of v7, /device:TPU:33, one launch (start us, length us, event | category | flops | bytes accessed | tf_op | source)
XLA Modules:
  0.0 131.2 jit_solution(15362176378089556823)
XLA Ops:
  0.0 127.1 %shard_map.73 = (bf16[8,512,256]{2,1,0:T(8,128)(2,1)}, f32[512,128]{1,0:T(8,128)}) custom-call(bf16[512,2048]{1,0:T(8,128)(2,1)} %tok.3, f32[1,2048]{1,0:T(1,128)} %bitcast.6, f32[64,1024]{1,0:T(8,128)} %up_w_in.1, f32[1,1024]{1,0:T(1,128)} %bitcast.8, f32[64,1024]{1,0:T(8,128)} %bitcast.5, f32[1,64]{1,0:T(1,128)} %bitcast.9), custom_call_target="tpu_custom_call" | custom-call | tf_op jit(solution)/shard_map/pallas_call | solution.py:431
  127.1 4.1 %shard_map.74 = bf16[512,2048]{1,0:T(8,128)(2,1)} custom-call(bf16[8,512,256]{2,1,0:T(8,128)(2,1)} %get-tuple-element.7.branch, f32[512,128]{1,0:T(8,128)} %get-tuple-element.8.scale, bf16[512,2048]{1,0:T(8,128)(2,1)} %tok.3, f32[1,2048]{1,0:T(1,128)} %bitcast.7), custom_call_target="tpu_custom_call" | custom-call | tf_op jit(solution)/shard_map/pallas_call | solution.py:491

commit v8 on v7

--- a/solution.py
+++ b/solution.py
@@ -10,9 +10,10 @@
 epsilon = 1e-06
 MESH = pl.DeviceIdType.MESH
 
-LAG = (8, 6)
+LAG = (10, 6)
 UP_PARTS, DOWN_PARTS = 4, 2
 TICKS = (4, 2)
+EARLY = (5, 6)
 TOKEN_PARTS = 4
 FINISH_PARTS = 4
 LIFTS = ((1, 8, 2, 7, 6, 5, 3, 4), (1, 8, 2, 7, 3, 6, 5, 4))
@@ -65,7 +66,7 @@
     z_quad = z // 4
     last = jnp.where(c == 0, reach[0], reach[1])
     lag = jnp.where(c == 0, LAG[0], LAG[1])
-    near = (z < nz // 2) | (c == 1)
+    near = (z < nz * 3 // 4) | (c == 1)
 
     def peer(i):
         return lax.rem(x + i, nx)
@@ -276,6 +277,7 @@
 
     ready = jnp.where(c == 0, 1, 0)
     ticks_at = jnp.where(c == 0, TICKS[0], TICKS[1])
+    early = jnp.where(c == 0, EARLY[0], EARLY[1])
 
     def lifts_at(over):
         return jnp.where((c == 1) & (over > 0), n_quads, jnp.clip(2 * over + 4, 0, n_quads))
@@ -311,11 +313,11 @@
         def _():
             activate()
 
-        @pl.when(near & (over > ready))
+        @pl.when(near & (over > ready) & (over <= ready + early))
         def _():
             lax.fori_loop(2 * (over - ready) - 2, 2 * (over - ready), project, 0)
 
-        @pl.when(near & home & (over >= ticks_at))
+        @pl.when(near & home & (over >= ticks_at) & (over < ticks_at + early))
         def _():
             lax.fori_loop(2 * (over - ticks_at) + 1, 2 * (over - ticks_at) + 3, tick, 0)
 
@@ -328,8 +330,8 @@
         lax.fori_loop(0, n_quads, lift, 0)
         activate()
 
-    made = jnp.where(near, 2 * (lag - ready), 0)
-    ticked = jnp.where(near, 2 * (lag - ticks_at + 1) + 1, 0)
+    made = jnp.where(near, 2 * early, 0)
+    ticked = jnp.where(near, 2 * jnp.minimum(early, lag - ticks_at + 1) + 1, 0)
 
     def output_pass(i, _):
         @pl.when(made + i < n_chunks)

time: 131 us -> 140 us (1.069)
  Pallas kernels: 131 us -> 139 us
    pallas_call x1, Pallas kernels: 127 us -> 135 us  [on_device(): pl.pallas_call(functools.partial(kernel, nz, nx), out_shape=(jax.ShapeDty...]
where the time goes in v8:
time: 140 us; the launch traced here: 139 us
  Pallas kernels  139 us (99%)
    pallas_call x1, Pallas kernels, on_device(): pl.pallas_call(functools.partial(kernel, nz, nx), out_shape=(jax.ShapeDty...  135 us
    pallas_call x1, Pallas kernels, on_device(): pl.pallas_call(finish, out_shape=jax.ShapeDtypeStruct((rows, width), bf16...  4.06 us

profile of v8, /device:TPU:33, one launch (start us, length us, event | category | flops | bytes accessed | tf_op | source)
XLA Modules:
  0.0 139.4 jit_solution(4374449056904802725)
XLA Ops:
  0.0 135.3 %shard_map.73 = (bf16[8,512,256]{2,1,0:T(8,128)(2,1)}, f32[512,128]{1,0:T(8,128)}) custom-call(bf16[512,2048]{1,0:T(8,128)(2,1)} %tok.3, f32[1,2048]{1,0:T(1,128)} %bitcast.6, f32[64,1024]{1,0:T(8,128)} %up_w_in.1, f32[1,1024]{1,0:T(1,128)} %bitcast.8, f32[64,1024]{1,0:T(8,128)} %bitcast.5, f32[1,64]{1,0:T(1,128)} %bitcast.9), custom_call_target="tpu_custom_call" | custom-call | tf_op jit(solution)/shard_map/pallas_call | solution.py:433
  135.3 4.1 %shard_map.74 = bf16[512,2048]{1,0:T(8,128)(2,1)} custom-call(bf16[8,512,256]{2,1,0:T(8,128)(2,1)} %get-tuple-element.7.branch, f32[512,128]{1,0:T(8,128)} %get-tuple-element.8.scale, bf16[512,2048]{1,0:T(8,128)(2,1)} %tok.3, f32[1,2048]{1,0:T(1,128)} %bitcast.7), custom_call_target="tpu_custom_call" | custom-call | tf_op jit(solution)/shard_map/pallas_call | solution.py:493

commit v9 on v8

--- a/solution.py
+++ b/solution.py
@@ -10,10 +10,10 @@
 epsilon = 1e-06
 MESH = pl.DeviceIdType.MESH
 
-LAG = (10, 6)
+LAG = (8, 6)
 UP_PARTS, DOWN_PARTS = 4, 2
-TICKS = (4, 2)
-EARLY = (5, 6)
+TICKS = (3, 1)
+EARLY = (6, 6)
 TOKEN_PARTS = 4
 FINISH_PARTS = 4
 LIFTS = ((1, 8, 2, 7, 6, 5, 3, 4), (1, 8, 2, 7, 3, 6, 5, 4))
@@ -313,9 +313,9 @@
         def _():
             activate()
 
-        @pl.when(near & (over > ready) & (over <= ready + early))
-        def _():
-            lax.fori_loop(2 * (over - ready) - 2, 2 * (over - ready), project, 0)
+        @pl.when(near & (over >= ready) & (over < ready + early))
+        def _():
+            lax.fori_loop(2 * (over - ready), 2 * (over - ready) + 2, project, 0)
 
         @pl.when(near & home & (over >= ticks_at) & (over < ticks_at + early))
         def _():

time: 140 us -> 131 us (0.936)
  Pallas kernels: 139 us -> 131 us
    pallas_call x1, Pallas kernels: 135 us -> 127 us  [on_device(): pl.pallas_call(functools.partial(kernel, nz, nx), out_shape=(jax.ShapeDty...]
where the time goes in v9:
time: 131 us
  Pallas kernels  131 us (100%)
    pallas_call x1, Pallas kernels, on_device(): pl.pallas_call(functools.partial(kernel, nz, nx), out_shape=(jax.ShapeDty...  127 us
    pallas_call x1, Pallas kernels, on_device(): pl.pallas_call(finish, out_shape=jax.ShapeDtypeStruct((rows, width), bf16...  4.06 us

profile of v9, /device:TPU:33, one launch (start us, length us, event | category | flops | bytes accessed | tf_op | source)
XLA Modules:
  0.0 130.7 jit_solution(4835502871684540565)
XLA Ops:
  0.0 126.6 %shard_map.73 = (bf16[8,512,256]{2,1,0:T(8,128)(2,1)}, f32[512,128]{1,0:T(8,128)}) custom-call(bf16[512,2048]{1,0:T(8,128)(2,1)} %tok.3, f32[1,2048]{1,0:T(1,128)} %bitcast.6, f32[64,1024]{1,0:T(8,128)} %up_w_in.1, f32[1,1024]{1,0:T(1,128)} %bitcast.8, f32[64,1024]{1,0:T(8,128)} %bitcast.5, f32[1,64]{1,0:T(1,128)} %bitcast.9), custom_call_target="tpu_custom_call" | custom-call | tf_op jit(solution)/shard_map/pallas_call | solution.py:433
  126.6 4.1 %shard_map.74 = bf16[512,2048]{1,0:T(8,128)(2,1)} custom-call(bf16[8,512,256]{2,1,0:T(8,128)(2,1)} %get-tuple-element.7.branch, f32[512,128]{1,0:T(8,128)} %get-tuple-element.8.scale, bf16[512,2048]{1,0:T(8,128)(2,1)} %tok.3, f32[1,2048]{1,0:T(1,128)} %bitcast.7), custom_call_target="tpu_custom_call" | custom-call | tf_op jit(solution)/shard_map/pallas_call | solution.py:493

commit v10 on v9

--- a/solution.py
+++ b/solution.py
@@ -11,7 +11,7 @@
 MESH = pl.DeviceIdType.MESH
 
 LAG = (8, 6)
-UP_PARTS, DOWN_PARTS = 4, 2
+UP_PARTS, DOWN_PARTS = 2, 2
 TICKS = (3, 1)
 EARLY = (6, 6)
 TOKEN_PARTS = 4

time: 131 us -> 131 us (level)
  no operation moved by 1% of the time
where the time goes in v10:
time: 131 us
  Pallas kernels  131 us (100%)
    pallas_call x1, Pallas kernels, on_device(): pl.pallas_call(functools.partial(kernel, nz, nx), out_shape=(jax.ShapeDty...  127 us
    pallas_call x1, Pallas kernels, on_device(): pl.pallas_call(finish, out_shape=jax.ShapeDtypeStruct((rows, width), bf16...  4.06 us

profile of v10, /device:TPU:33, one launch (start us, length us, event | category | flops | bytes accessed | tf_op | source)
XLA Modules:
  0.0 131.2 jit_solution(12630199504934617912)
XLA Ops:
  0.0 127.2 %shard_map.73 = (bf16[8,512,256]{2,1,0:T(8,128)(2,1)}, f32[512,128]{1,0:T(8,128)}) custom-call(bf16[512,2048]{1,0:T(8,128)(2,1)} %tok.3, f32[1,2048]{1,0:T(1,128)} %bitcast.6, f32[64,1024]{1,0:T(8,128)} %up_w_in.1, f32[1,1024]{1,0:T(1,128)} %bitcast.8, f32[64,1024]{1,0:T(8,128)} %bitcast.5, f32[1,64]{1,0:T(1,128)} %bitcast.9), custom_call_target="tpu_custom_call" | custom-call | tf_op jit(solution)/shard_map/pallas_call | solution.py:433
  127.2 4.1 %shard_map.74 = bf16[512,2048]{1,0:T(8,128)(2,1)} custom-call(bf16[8,512,256]{2,1,0:T(8,128)(2,1)} %get-tuple-element.7.branch, f32[512,128]{1,0:T(8,128)} %get-tuple-element.8.scale, bf16[512,2048]{1,0:T(8,128)(2,1)} %tok.3, f32[1,2048]{1,0:T(1,128)} %bitcast.7), custom_call_target="tpu_custom_call" | custom-call | tf_op jit(solution)/shard_map/pallas_call | solution.py:493
